TPU v7x, 32 devices: a whole 2x2x4 slice. The times are simulated.
32 devices in a mesh: ep: 8 (over z, x), tp: 4 (over y, core).
Axes of the slice: x: 2, y: 2, z: 4, core: 2. Of those that a mesh axis runs over, the one named last changes fastest.
Arguments:
- queries: bfloat16 [1024, 1024], P('ep', 'tp'), may hold values from -6 to 6
- key_states: bfloat16 [1024, 256], P('ep'), may hold values from -192 to 192
- value_states: bfloat16 [1024, 256], P('ep'), may hold values from -12 to 12
- sink_logit: float32 [16], P('tp'), may hold values from 3 to 7
- out_weight: bfloat16 [1024, 2048], P('tp'), may hold values from -0.1875 to 0.1875
- expert_input: bfloat16 [1024, 2048], P('ep'), may hold values from -6 to 6
- norm_gain: float32 [2048], replicated, may hold values from 0.1 to 1.9
- routes: int32 [1024, 2], P('ep'), may hold values from 0 to 7, all different within a row; in each aligned block of 128 rows (0 to 127, 128 to 255, ...) at most 40 rows name the same one
- route_weight: float32 [1024, 2], P('ep'), may hold values from 0.1 to 1
- gate_weight: bfloat16 [8, 2048, 4096], P('ep', None, 'tp'), may hold values from -0.125 to 0.125
- up_weight: bfloat16 [8, 2048, 4096], P('ep', None, 'tp'), may hold values from -0.125 to 0.125
- down_weight: bfloat16 [8, 4096, 2048], P('ep', 'tp'), may hold values from -0.125 to 0.125
Outputs:
- mixer_out: bfloat16 [1024, 2048], P(('ep', 'tp'))
- expert_out: bfloat16 [1024, 2048], P('ep', 'tp')
Inputs may be any that keep to these rules, and one draw needn't show every extreme that they name: `routes`: each row names 2 different experts. Within the rows of one index of ep (aligned blocks of 128 rows) no expert is named more than 40 times, a bound that some blocks reach.
All inputs are finite; a program needn't handle non-finite values.
Results may differ from a plain program's by a relative error of at most 0.025.
Values may be sent and summed in bfloat16 or wider, within the bound.
A program may use at most 64 MiB of HBM per device.

v0:
```python
import functools

import jax
import jax.numpy as jnp
from jax import lax
from jax.experimental import pallas as pl
from jax.experimental.pallas import tpu as pltpu
from jax.sharding import PartitionSpec as P

HEADS = 16
KV_HEADS = 4
HEAD_DIM = 64
WINDOW = 128
TOP = 2


NORM_EPSILON = 1e-05
ROTARY_BASE = 500000.0
MASK_VALUE = -1e30


def layer_norm(activations, norm_gain):
    values = activations.astype(jnp.float32)
    average = jnp.mean(values, axis=-1, keepdims=True)
    centred = values - average
    variance = jnp.mean(centred * centred, axis=-1, keepdims=True)
    return (centred * lax.rsqrt(variance + NORM_EPSILON) * norm_gain).astype(jnp.bfloat16)


def rotate(head_rows, positions):
    half_dim = head_rows.shape[-1] // 2
    exponent = jnp.arange(half_dim, dtype=jnp.float32) * (2.0 / head_rows.shape[-1])
    frequency = jnp.power(jnp.float32(ROTARY_BASE), -exponent)
    angles = positions.astype(jnp.float32)[:, None] * frequency[None, :]
    cosine = jnp.cos(angles)[:, None, :]
    sine_part = jnp.sin(angles)[:, None, :]
    first_half = head_rows[..., :half_dim].astype(jnp.float32)
    second_half = head_rows[..., half_dim:].astype(jnp.float32)
    turned = jnp.concatenate(
        [
            first_half * cosine - second_half * sine_part,
            second_half * cosine + first_half * sine_part,
        ],
        axis=-1,
    )
    return turned.astype(jnp.bfloat16)


def fused_kernel(
    sizes,
    query_ref,
    kv_ref,
    sink_ref,
    input_ref,
    gain_ref,
    routes_ref,
    route_weight_ref,
    out_hbm,
    gate_hbm,
    up_hbm,
    down_hbm,
    mixer_ref,
    expert_ref,
    out_w,
    gate_w,
    up_w,
    down_w,
    low_kv,
    high_kv,
    packed,
    rows_in,
    hidden,
    mix_send,
    mix_recv,
    half_send,
    half_recv,
    cross_send,
    cross_recv,
    final_send,
    returned,
    own_total,
    load_sem,
    halo_send_sem,
    halo_recv_sem,
    row_send_sem,
    row_recv_sem,
    forward_send_sem,
    forward_recv_sem,
    mix_send_sem,
    mix_recv_sem,
    half_send_sem,
    half_recv_sem,
    cross_send_sem,
    cross_recv_sem,
    final_send_sem,
    final_recv_sem,
):
    n_ep, n_tp, cap = sizes
    me, my_tp = lax.axis_index("ep"), lax.axis_index("tp")
    core = lax.rem(my_tp, 2)
    pair = my_tp // 2
    n_pair = n_tp // 2
    sibling = my_tp + 1 - 2 * core
    local_heads, row_count, head_dim = query_ref.shape

    loads = [
        pltpu.make_async_copy(source, target, load_sem.at[number])
        for number, (source, target) in enumerate(
            [(out_hbm, out_w), (gate_hbm.at[0], gate_w), (up_hbm.at[0], up_w), (down_hbm.at[0], down_w)]
        )
    ]

    def remote(source, target, send_sem, recv_sem, ep, tp):
        return pltpu.make_async_remote_copy(
            src_ref=source,
            dst_ref=target,
            send_sem=send_sem,
            recv_sem=recv_sem,
            device_id=(ep, tp),
            device_id_type=pl.DeviceIdType.MESH,
        )

    barrier = pltpu.get_barrier_semaphore()
    for step in range(1, n_ep):
        pl.semaphore_signal(
            barrier, inc=1, device_id=(lax.rem(me + step, n_ep), my_tp),
            device_id_type=pl.DeviceIdType.MESH,
        )
    for step in range(1, n_tp):
        pl.semaphore_signal(
            barrier, inc=1, device_id=(me, lax.rem(my_tp + step, n_tp)),
            device_id_type=pl.DeviceIdType.MESH,
        )
    for load in loads:
        load.start()

    half = input_ref.shape[1] // 2
    normed = layer_norm(input_ref[...], gain_ref[...])
    own_half = jnp.where(core == 0, normed[:, :half], normed[:, half:])
    diagonal = (
        lax.broadcasted_iota(jnp.int32, (row_count, row_count), 0)
        == lax.broadcasted_iota(jnp.int32, (row_count, row_count), 1)
    )

    def column(ref, k):
        return jnp.sum(
            jnp.where(diagonal, ref[k : k + 1, :].astype(jnp.float32), 0.0),
            axis=1, keepdims=True,
        )

    routes = [column(routes_ref, k).astype(jnp.int32) for k in range(TOP)]
    experts = lax.broadcasted_iota(jnp.int32, (row_count, 128), 1)
    named = [(routes[k] == experts).astype(jnp.float32) for k in range(TOP)]
    earlier = (
        lax.broadcasted_iota(jnp.int32, (row_count, row_count), 0)
        > lax.broadcasted_iota(jnp.int32, (row_count, row_count), 1)
    )
    ahead = jnp.dot(
        earlier.astype(jnp.float32).astype(jnp.bfloat16),
        functools.reduce(jnp.add, named).astype(jnp.bfloat16),
        preferred_element_type=jnp.float32,
    )
    slot_numbers = lax.broadcasted_iota(jnp.int32, (row_count, n_ep * cap), 1)
    onehot = jnp.zeros((row_count, n_ep * cap), jnp.float32)
    combine = jnp.zeros((row_count, n_ep * cap), jnp.float32)
    for k in range(TOP):
        rank = jnp.sum(ahead * named[k], axis=1, keepdims=True).astype(jnp.int32)
        chosen = slot_numbers == routes[k] * cap + rank
        onehot = jnp.where(chosen, 1.0, onehot)
        combine = jnp.where(chosen, column(route_weight_ref, k), combine)
    combine = combine.astype(jnp.bfloat16)
    slots = lax.dot_general(
        onehot.astype(jnp.bfloat16), own_half, (((0,), (0,)), ((), ())),
        preferred_element_type=jnp.float32,
    )
    packed[...] = slots.astype(jnp.bfloat16).reshape(packed.shape)
    rows_in[core, me] = packed[me]
    pl.semaphore_wait(barrier, n_ep + n_tp - 2)

    right, left = lax.rem(me + 1, n_ep), lax.rem(me + n_ep - 1, n_ep)
    halos = [
        remote(kv_ref.at[:, pl.ds(row_count - WINDOW, WINDOW)], low_kv,
               halo_send_sem.at[0], halo_recv_sem.at[0], right, my_tp),
        remote(kv_ref.at[:, pl.ds(0, WINDOW)], high_kv,
               halo_send_sem.at[1], halo_recv_sem.at[1], left, my_tp),
    ]
    for halo in halos:
        halo.start()
    sends = []
    for step in range(1, n_ep):
        target = lax.rem(me + step, n_ep)
        sends.append(
            remote(packed.at[target], rows_in.at[core, me],
                   row_send_sem.at[step], row_recv_sem.at[step], target, my_tp)
        )
        sends[-1].start()
    forwards = [
        remote(packed.at[me], rows_in.at[core, me],
               forward_send_sem.at[0], forward_recv_sem.at[0], me, sibling)
    ]
    forwards[0].start()

    for halo in halos:
        halo.wait()
    keys = jnp.concatenate([low_kv[0], kv_ref[0], high_kv[0]], axis=0)
    values = jnp.concatenate([low_kv[1], kv_ref[1], high_kv[1]], axis=0)
    query = query_ref[...].reshape(local_heads * row_count, head_dim)
    scores = lax.dot_general(
        query, keys, (((1,), (1,)), ((), ())), preferred_element_type=jnp.float32
    ) * head_dim ** (-0.5)
    local = lax.rem(lax.broadcasted_iota(jnp.int32, scores.shape, 0), row_count)
    other = lax.broadcasted_iota(jnp.int32, scores.shape, 1) - WINDOW
    position = me * row_count + other
    allowed = (
        (jnp.abs(local - other) <= WINDOW) & (position >= 0) & (position < row_count * n_ep)
    )
    scores = jnp.where(allowed, scores, MASK_VALUE)
    head_number = lax.broadcasted_iota(jnp.int32, (scores.shape[0], 1), 0) // row_count
    sinks = jnp.zeros(head_number.shape, jnp.float32)
    for head in range(local_heads):
        sinks = jnp.where(head_number == head, sink_ref[head], sinks)
    largest = jnp.maximum(jnp.max(scores, axis=-1, keepdims=True), sinks)
    weights = jnp.exp(scores - largest)
    denominator = jnp.sum(weights, axis=-1, keepdims=True) + jnp.exp(sinks - largest)
    probability = (weights / denominator).astype(jnp.bfloat16)
    attended = jnp.dot(probability, values, preferred_element_type=jnp.float32)
    attended = attended.astype(jnp.bfloat16)

    for step in range(1, n_ep):
        source = lax.rem(me + n_ep - step, n_ep)
        remote(packed.at[source], rows_in.at[core, source],
               row_send_sem.at[step], row_recv_sem.at[step], source, my_tp).wait_recv()
        forwards.append(
            remote(rows_in.at[core, source], rows_in.at[core, source],
                   forward_send_sem.at[step], forward_recv_sem.at[step], me, sibling)
        )
        forwards[-1].start()

    loads[0].wait()
    partial_sum = jnp.zeros((row_count, out_w.shape[1]), jnp.float32)
    for head in range(local_heads):
        partial_sum += jnp.dot(
            attended[head * row_count : (head + 1) * row_count],
            out_w[pl.ds(head * head_dim, head_dim), :],
            preferred_element_type=jnp.float32,
        )
    mix_send[...] = partial_sum.reshape(mix_send.shape).astype(jnp.bfloat16)
    for step in range(1, n_tp):
        target = lax.rem(my_tp + step, n_tp)
        sends.append(
            remote(mix_send.at[target], mix_recv.at[step - 1],
                   mix_send_sem.at[step - 1], mix_recv_sem.at[step - 1], me, target)
        )
        sends[-1].start()

    loads[1].wait()
    loads[2].wait()
    for forward in forwards:
        forward.wait_recv()
    width = gate_w.shape[1]
    tile = min(width, 512)
    total_rows = n_ep * cap

    @pl.loop(0, width // tile)
    def _(number):
        columns = pl.ds(pl.multiple_of(number * tile, tile), tile)
        gate_act = jnp.zeros((total_rows, tile), jnp.float32)
        up_act = jnp.zeros((total_rows, tile), jnp.float32)
        for side in range(2):
            block = rows_in[side].reshape(total_rows, half)
            rows = pl.ds(side * half, half)
            gate_act += jnp.dot(block, gate_w[rows, columns], preferred_element_type=jnp.float32)
            up_act += jnp.dot(block, up_w[rows, columns], preferred_element_type=jnp.float32)
        hidden[:, columns] = (gate_act / (1.0 + jnp.exp(-gate_act)) * up_act).astype(jnp.bfloat16)

    loads[3].wait()
    out_width = expert_ref.shape[1]

    def down_slice(owner):
        columns = pl.ds(pl.multiple_of(owner * out_width, out_width), out_width)
        return jnp.dot(hidden[...], down_w[:, columns], preferred_element_type=jnp.float32)

    pair_sends, crosses, returns = [], [], []
    order = [lax.rem(me + 1 + place, n_ep) for place in range(n_ep)]
    for step in range(n_pair):
        number = lax.rem(pair + step + 1, n_pair)
        half_send[step] = (
            down_slice(2 * number + 1 - core).astype(jnp.bfloat16).reshape(n_ep, cap, out_width)
        )
        exchange = [
            remote(half_send.at[step, source], half_recv.at[step, source],
                   half_send_sem.at[step, place], half_recv_sem.at[step, place], me, sibling)
            for place, source in enumerate(order)
        ]
        for copy in exchange:
            copy.start()
        pair_sends += exchange
        own_total[...] = down_slice(2 * number + core).reshape(n_ep, cap, out_width)
        for place, source in enumerate(order):
            exchange[place].wait_recv()
            own = own_total[source] + half_recv[step, source].astype(jnp.float32)
            if step < n_pair - 1:
                cross_send[step, source] = own.astype(jnp.bfloat16)
                crosses.append(
                    remote(cross_send.at[step, source], cross_recv.at[step, source],
                           cross_send_sem.at[step, place], cross_recv_sem.at[step, place],
                           me, 2 * number + core)
                )
                crosses[-1].start()
                continue
            for other in range(n_pair - 1):
                crosses[other * n_ep + place].wait_recv()
                own += cross_recv[other, source].astype(jnp.float32)
            if place == n_ep - 1:
                returned[me] = own.astype(jnp.bfloat16)
                continue
            final_send[source] = own.astype(jnp.bfloat16)
            returns.append(
                remote(final_send.at[source], returned.at[me],
                       final_send_sem.at[place], final_recv_sem.at[place], source, my_tp)
            )
            returns[-1].start()

    mixed = mix_send[my_tp].astype(jnp.float32)
    for step in range(1, n_tp):
        sends[n_ep - 2 + step].wait_recv()
        mixed += mix_recv[step - 1].astype(jnp.float32)
    mixer_ref[...] = mixed

    for copy in returns:
        copy.wait_recv()
    expert_ref[...] = jnp.dot(
        combine, returned[...].reshape(total_rows, out_width),
        preferred_element_type=jnp.float32,
    )
    for copy in sends + forwards + pair_sends + crosses + returns:
        copy.wait_send()


def on_device(
    queries,
    key_states,
    value_states,
    sink_logit,
    out_weight,
    expert_input,
    norm_gain,
    routes,
    route_weight,
    gate_weight,
    up_weight,
    down_weight,
):
    expert_devices = lax.axis_size("ep")
    group_devices = lax.axis_size("tp")
    expert_index = lax.axis_index("ep")
    tensor_index = lax.axis_index("tp")
    row_count = queries.shape[0]
    local_heads = queries.shape[1] // HEAD_DIM
    group_size = HEADS // KV_HEADS
    positions = expert_index * row_count + jnp.arange(row_count, dtype=jnp.int32)
    turned_query = rotate(queries.reshape(row_count, local_heads, HEAD_DIM), positions)
    shared_head = tensor_index * local_heads // group_size
    own_key = lax.dynamic_slice_in_dim(key_states, shared_head * HEAD_DIM, HEAD_DIM, 1)
    own_value = lax.dynamic_slice_in_dim(value_states, shared_head * HEAD_DIM, HEAD_DIM, 1)
    turned_key = rotate(own_key.reshape(row_count, 1, HEAD_DIM), positions).reshape(
        row_count, HEAD_DIM
    )
    token_count = expert_input.shape[0]
    expert_count = expert_devices * gate_weight.shape[0]
    capacity = token_count * TOP * 5 // (4 * expert_count)
    rows_per_slot = -(-capacity // 16) * 16
    slot_count = expert_count * rows_per_slot
    width = expert_input.shape[1]
    out_width = width // group_devices
    hidden_width = gate_weight.shape[2]
    mix_rows = row_count // group_devices
    n_pair = group_devices // 2
    vmem = pl.BlockSpec(memory_space=pltpu.VMEM)
    hbm = pl.BlockSpec(memory_space=pl.ANY)
    bf16 = jnp.bfloat16
    dma = pltpu.SemaphoreType.DMA
    mixer_out, expert_out = pl.pallas_call(
        functools.partial(fused_kernel, (expert_devices, group_devices, rows_per_slot)),
        out_shape=(
            jax.ShapeDtypeStruct((mix_rows, width), jnp.float32),
            jax.ShapeDtypeStruct((token_count, out_width), jnp.float32),
        ),
        in_specs=[vmem] * 2 + [pl.BlockSpec(memory_space=pltpu.SMEM)] + [vmem] * 4 + [hbm] * 4,
        out_specs=(vmem, vmem),
        scratch_shapes=[
            pltpu.VMEM(out_weight.shape, bf16),
            pltpu.VMEM(gate_weight.shape[1:], bf16),
            pltpu.VMEM(up_weight.shape[1:], bf16),
            pltpu.VMEM(down_weight.shape[1:], bf16),
            pltpu.VMEM((2, WINDOW, HEAD_DIM), bf16),
            pltpu.VMEM((2, WINDOW, HEAD_DIM), bf16),
            pltpu.VMEM((expert_devices, rows_per_slot, width // 2), bf16),
            pltpu.VMEM((2, expert_devices, rows_per_slot, width // 2), bf16),
            pltpu.VMEM((slot_count, hidden_width), bf16),
            pltpu.VMEM((group_devices, mix_rows, width), bf16),
            pltpu.VMEM((group_devices - 1, mix_rows, width), bf16),
            pltpu.VMEM((n_pair, expert_devices, rows_per_slot, out_width), bf16),
            pltpu.VMEM((n_pair, expert_devices, rows_per_slot, out_width), bf16),
            pltpu.VMEM((n_pair, expert_devices, rows_per_slot, out_width), bf16),
            pltpu.VMEM((n_pair, expert_devices, rows_per_slot, out_width), bf16),
            pltpu.VMEM((expert_devices, rows_per_slot, out_width), bf16),
            pltpu.VMEM((expert_devices, rows_per_slot, out_width), bf16),
            pltpu.VMEM((expert_devices, rows_per_slot, out_width), jnp.float32),
            dma((4,)),
            dma((2,)),
            dma((2,)),
            dma((expert_devices,)),
            dma((expert_devices,)),
            dma((expert_devices,)),
            dma((expert_devices,)),
            dma((group_devices,)),
            dma((group_devices,)),
            dma((n_pair, expert_devices)),
            dma((n_pair, expert_devices)),
            dma((n_pair, expert_devices)),
            dma((n_pair, expert_devices)),
            dma((expert_devices,)),
            dma((expert_devices,)),
        ],
        compiler_params=pltpu.CompilerParams(
            collective_id=0, has_side_effects=True, vmem_limit_bytes=56 * 1024 * 1024
        ),
    )(
        turned_query.transpose(1, 0, 2),
        jnp.stack([turned_key, own_value]),
        sink_logit,
        expert_input,
        norm_gain[None, :],
        routes.T,
        route_weight.T,
        out_weight,
        gate_weight,
        up_weight,
        down_weight,
    )
    return (mixer_out.astype(bf16), expert_out.astype(bf16))


def solution(mesh):
    in_specs = (
        P("ep", "tp"),
        P("ep", None),
        P("ep", None),
        P("tp"),
        P("tp", None),
        P("ep", None),
        P(),
        P("ep", None),
        P("ep", None),
        P("ep", None, "tp"),
        P("ep", None, "tp"),
        P("ep", "tp", None),
    )
    out_specs = (P(("ep", "tp"), None), P("ep", "tp"))
    return jax.shard_map(
        on_device, mesh=mesh, in_specs=in_specs, out_specs=out_specs, check_vma=False
    )
```

profile of v0, /device:TPU:0, one launch (start us, length us, event | category | flops | bytes accessed | tf_op | source)
XLA Modules:
  0.0 55.3 jit_solution(11847671934959606128)
XLA Ops:
  0.7 0.9 %dynamic-slice_bitcast_fusion = (bf16[1,128,64]{2,1,0:T(8,128)(2,1)S(1)}, bf16[128,1,64]{2,0,1:T(8,128)(2,1)S(1)}) fusion(bf16[128,256]{1,0:T(8,128)(2,1)} %param.14, s32[]{:T(128)S(6)} %select_n.10, bf16[128,256]{1,0:T(8,128)(2,1)} %param.13), kind=kLoop, calls=%fused_computation.23 | loop fusion | bytes 65540 | tf_op jit(solution)/shard_map/stack | solution.py:431
  1.6 1.0 %copy.17 = bf16[128,256]{0,1:T(8,128)(2,1)S(1)} copy(bf16[128,256]{1,0:T(8,128)(2,1)} %param.12) | data formatting | bytes 131072 | tf_op args[0]
  2.5 0.3 fusion.13
  2.9 0.7 %pad_maximum_fusion.kv_ref = bf16[2,128,64]{2,1,0:T(8,128)(2,1)} fusion(bf16[1,128,64]{2,1,0:T(8,128)(2,1)S(1)} %get-tuple-element.14, bf16[1,128,32]{2,1,0:T(8,128)(2,1)S(1)} %get-tuple-element.11, bf16[1,128,32]{2,1,0:T(8,128)(2,1)S(1)} %get-tuple-element.10), kind=kLoop, calls=%fused_computation.19 | loop fusion | flops 98304 | bytes 65536 | tf_op jit(solution)/shard_map/stack | solution.py:431
  3.6 0.3 multiply_cosine_fusion.1
  3.9 0.1 copy.21
  4.0 0.1 copy.18
  4.2 0.1 fusion.1
  4.2 0.8 %maximum_bitcast_fusion.query_ref = bf16[4,128,64]{2,1,0:T(8,128)(2,1)} fusion(bf16[128,4,32]{2,0,1:T(8,128)(2,1)S(1)} %get-tuple-element.7, bf16[128,4,32]{2,0,1:T(8,128)(2,1)S(1)} %get-tuple-element.6), kind=kLoop, calls=%fused_computation.6 | loop fusion | flops 131072 | bytes 131072 | tf_op jit(solution)/shard_map/transpose | solution.py:430
  5.0 47.0 %shard_map.131 = (f32[32,2048]{1,0:T(8,128)}, f32[128,512]{1,0:T(8,128)}) custom-call(bf16[4,128,64]{2,1,0:T(8,128)(2,1)} %maximum_bitcast_fusion.query_ref, bf16[2,128,64]{2,1,0:T(8,128)(2,1)} %pad_maximum_fusion.kv_ref, f32[4]{0:T(128)} %sink_ref.1, bf16[128,2048]{1,0:T(8,128)(2,1)} %input_ref.1, f32[1,2048]{1,0:T(1,128)} %bitcast.15, s32[2,128]{1,0:T(2,128)} %bitcast.16, ...), custom_call_target="tpu_custom_call" | custom-call | tf_op jit(solution)/shard_map/pallas_call | solution.py:383
  52.0 1.6 %convert_element_type.42 = bf16[32,2048]{1,0:T(8,128)(2,1)} convert(f32[32,2048]{1,0:T(8,128)} %get-tuple-element.4) | non-fusion elementwise | flops 65536 | bytes 393216 | tf_op jit(solution)/shard_map/convert_element_type | solution.py:442
  53.6 1.6 %convert_element_type.43 = bf16[128,512]{1,0:T(8,128)(2,1)} convert(f32[128,512]{1,0:T(8,128)} %get-tuple-element.5) | non-fusion elementwise | flops 65536 | bytes 393216 | tf_op jit(solution)/shard_map/convert_element_type | solution.py:442
  (3 shorter events, 0.0 us)
where the time goes:
time: 55.6 us; the launch traced here: 55.3 us
  Pallas kernels  47 us (85%)
  other arithmetic  5.46 us (10%)
  local copies, waits for them, and re-layouts  2.08 us (4%)
  between operations  0.72 us (1%)
    pallas_call x1, Pallas kernels, on_device(): pl.pallas_call(functools.partial(fused_kernel, (expert_devices, group_dev...  47 us
    convert_element_type x2, other arithmetic, on_device(): return (mixer_out.astype(bf16), expert_out.astype(bf16))  3.24 us

commit v1 on v0

v1 whole, which is shorter than its diff:
```python
import functools

import jax
import jax.numpy as jnp
import numpy as np
from jax import lax
from jax.experimental import pallas as pl
from jax.experimental.pallas import tpu as pltpu
from jax.sharding import PartitionSpec as P

HEADS = 16
KV_HEADS = 4
HEAD_DIM = 64
WINDOW = 128
TOP = 2
LANES = 128


NORM_EPSILON = 1e-05
ROTARY_BASE = 500000.0
MASK_VALUE = -1e30


def layer_norm(activations, norm_gain):
    values = activations.astype(jnp.float32)
    average = jnp.mean(values, axis=-1, keepdims=True)
    centred = values - average
    variance = jnp.mean(centred * centred, axis=-1, keepdims=True)
    return (centred * lax.rsqrt(variance + NORM_EPSILON) * norm_gain).astype(jnp.bfloat16)


def angle_table(row_count, blocks):
    lane = np.arange(LANES) % HEAD_DIM
    half_dim = HEAD_DIM // 2
    frequency = ROTARY_BASE ** (-2.0 * (lane % half_dim) / HEAD_DIM)
    sign = np.where(lane < half_dim, -1.0, 1.0)
    rows = np.arange(row_count)[:, None] * frequency[None, :]
    bases = np.arange(blocks)[:, None] * row_count * frequency[None, :]
    return np.concatenate(
        [np.cos(rows), sign * np.sin(rows), np.cos(bases), sign * np.sin(bases)]
    ).astype(np.float32)


def partner(index, mask):
    flipped, bit = index, 1
    while bit <= mask:
        if mask & bit:
            flipped = flipped + bit * (1 - 2 * lax.rem(index // bit, 2))
        bit *= 2
    return flipped


def fused_kernel(
    sizes,
    query_hbm,
    key_hbm,
    value_hbm,
    table_hbm,
    sink_hbm,
    input_hbm,
    gain_hbm,
    routes_hbm,
    route_weight_hbm,
    out_hbm,
    gate_hbm,
    up_hbm,
    down_hbm,
    mixer_ref,
    expert_ref,
    query_v,
    key_v,
    value_v,
    table_v,
    sink_v,
    input_v,
    gain_v,
    routes_v,
    route_weight_v,
    out_w,
    gate_w,
    up_w,
    down_w,
    normed_v,
    own_kv,
    halo_send,
    low_kv,
    high_kv,
    packed,
    rows_in,
    gathered,
    hidden,
    mix_send,
    mix_sib,
    mix_cross,
    mix_recv,
    sib_send,
    sib_recv,
    own_acc,
    cross_send,
    cross_recv,
    final_send,
    returned,
    combine_left,
    combine_right,
    load_sem,
    halo_send_sem,
    halo_recv_sem,
    send_sem,
    net_recv_sem,
    far_recv_sem,
    near_recv_sem,
    mix_sib_recv_sem,
    mix_recv_sem,
    sib_recv_sem,
    cross_recv_sem,
    final_recv_sem,
):
    n_ep, n_tp, main, tail = sizes
    cap = main + tail
    halves = 2 if tail else 1
    f32, bf16 = jnp.float32, jnp.bfloat16
    me, my_tp = lax.axis_index("ep"), lax.axis_index("tp")
    core = lax.rem(my_tp, 2)
    pair = my_tp // 2
    n_pair = n_tp // 2
    sibling = my_tp + 1 - 2 * core
    row_count, width = input_v.shape
    slice_width = width // n_tp
    piece = slice_width // halves
    head_dim = HEAD_DIM
    local_heads = sink_v.shape[1]
    half_count = n_ep // 2
    near = list(range(half_count))
    groups = [
        list(range(3 * n_ep // 4, n_ep)),
        list(range(half_count, 3 * n_ep // 4)),
        near,
    ]
    experts_of = [partner(me, k) for k in range(n_ep)]
    pair_up = [lax.rem(pair + p, n_pair) for p in range(n_pair)]
    pair_down = [lax.rem(pair + n_pair - p, n_pair) for p in range(n_pair)]

    names = [
        (routes_hbm, routes_v),
        (route_weight_hbm, route_weight_v),
        (gain_hbm, gain_v),
        (input_hbm, input_v),
        (table_hbm, table_v),
        (key_hbm, key_v),
        (value_hbm, value_v),
        (query_hbm, query_v),
        (out_hbm, out_w),
        (gate_hbm.at[0], gate_w),
        (up_hbm.at[0], up_w),
        (down_hbm.at[0], down_w),
        (sink_hbm, sink_v),
    ]
    shared = my_tp * local_heads // (HEADS // KV_HEADS)
    shared_sib = sibling * local_heads // (HEADS // KV_HEADS)
    block = pl.ds(pl.multiple_of(shared // 2 * LANES, LANES), LANES)
    names[5] = (key_hbm.at[:, block], key_v)
    names[6] = (value_hbm.at[:, block], value_v)
    loads = [
        pltpu.make_async_copy(source, target, load_sem.at[number])
        for number, (source, target) in enumerate(names)
    ]

    def remote(source, target, send_sem, recv_sem, ep, tp):
        return pltpu.make_async_remote_copy(
            src_ref=source,
            dst_ref=target,
            send_sem=send_sem,
            recv_sem=recv_sem,
            device_id=(ep, tp),
            device_id_type=pl.DeviceIdType.MESH,
        )

    barrier = pltpu.get_barrier_semaphore()
    for k in range(n_ep - 1, 0, -1):
        pl.semaphore_signal(
            barrier, inc=1, device_id=(experts_of[k], sibling),
            device_id_type=pl.DeviceIdType.MESH,
        )
    for step in range(1, n_tp):
        pl.semaphore_signal(
            barrier, inc=1, device_id=(me, lax.rem(my_tp + step, n_tp)),
            device_id_type=pl.DeviceIdType.MESH,
        )
    for load in loads:
        load.start()

    def start(copy):
        copy.start()

    def arrived(target, sem):
        pltpu.make_async_copy(target, target, sem).wait()

    loads[0].wait()
    routes = [routes_v[k : k + 1, :] for k in range(TOP)]
    expert_iota = lax.broadcasted_iota(jnp.int32, (n_ep, row_count), 0)
    named = [(routes[k] == expert_iota).astype(f32) for k in range(TOP)]
    earlier = (
        lax.broadcasted_iota(jnp.int32, (row_count, row_count), 0)
        < lax.broadcasted_iota(jnp.int32, (row_count, row_count), 1)
    )
    ahead = jnp.dot(
        functools.reduce(jnp.add, named).astype(bf16),
        earlier.astype(f32).astype(bf16),
        preferred_element_type=f32,
    )
    rank = [
        jnp.sum(ahead * named[k], axis=0, keepdims=True).astype(jnp.int32) for k in range(TOP)
    ]

    def slot_onehot(k):
        slot = lax.broadcasted_iota(jnp.int32, (cap, row_count), 0)
        chosen = [(jnp.where(routes[j] == experts_of[k], rank[j], -1) == slot) for j in range(TOP)]
        return functools.reduce(jnp.logical_or, chosen).astype(f32)

    def pack(values):
        if not tail:
            return values
        parts = [values[:main, :piece], values[:main, piece:], values[main:, :piece], values[main:, piece:]]
        return jnp.concatenate(parts, axis=0)

    order = [k for group in groups for k in group]
    far = [k for k in order if k >= half_count]
    close = [k for k in order if k < half_count]
    for number in range(4, 7):
        loads[number].wait()
    lane = lax.broadcasted_iota(jnp.int32, (row_count, LANES), 1)
    low_lane = lane < head_dim
    first_half = lax.rem(lane, head_dim) < head_dim // 2
    row_cos, row_sin = table_v[:row_count], table_v[row_count : 2 * row_count]
    base_cos = table_v[pl.ds(2 * row_count + me, 1), :]
    base_sin = table_v[pl.ds(2 * row_count + n_ep + me, 1), :]
    cosine = base_cos * row_cos - base_sin * row_sin
    sine = base_sin * row_cos + base_cos * row_sin

    def turn(values):
        values = values.astype(f32)
        other = jnp.where(
            first_half,
            pltpu.roll(values, LANES - head_dim // 2, 1),
            pltpu.roll(values, head_dim // 2, 1),
        )
        return values * cosine + other * sine

    turned = turn(key_v[...])
    value = value_v[...].astype(f32)
    turned_roll, value_roll = pltpu.roll(turned, head_dim, 1), pltpu.roll(value, head_dim, 1)

    def key_value(head):
        upper = lax.rem(head, 2) == 1
        return jnp.where(
            low_lane,
            jnp.where(upper, turned_roll, turned),
            jnp.where(upper, value, value_roll),
        ).astype(bf16)

    own_kv[...] = key_value(shared)
    halo_send[...] = key_value(shared_sib)
    to_right = remote(halo_send.at[pl.ds(row_count - WINDOW, WINDOW)], low_kv,
                      halo_send_sem.at[0], halo_recv_sem.at[0], lax.rem(me + 1, n_ep), sibling)
    to_left = remote(halo_send.at[pl.ds(0, WINDOW)], high_kv,
                     halo_send_sem.at[1], halo_recv_sem.at[1], lax.rem(me + n_ep - 1, n_ep), sibling)

    far_onehot = jnp.concatenate([slot_onehot(k) for k in far], axis=0).astype(bf16)
    close_onehot = jnp.concatenate([slot_onehot(k) for k in close], axis=0).astype(bf16)

    loads[2].wait()
    loads[3].wait()
    normed_v[...] = layer_norm(input_v[...], gain_v[...])

    def columns_of(owner, size):
        return pl.ds(pl.multiple_of(owner * size, size), size)

    own_slice = normed_v[:, columns_of(my_tp, slice_width)]
    slots = jnp.dot(far_onehot, own_slice, preferred_element_type=f32)
    for place, k in enumerate(far):
        packed[0, k] = pack(slots[place * cap : (place + 1) * cap]).astype(bf16)

    pl.semaphore_wait(barrier, n_ep + n_tp - 2)

    def net(k, q):
        owner = 2 * pair_up[q] + core
        return remote(packed.at[q, k], rows_in.at[owner, k],
                      send_sem.at[0 if k >= half_count else 1], net_recv_sem.at[k], experts_of[k], sibling)

    @pl.when(me < n_ep - 1)
    def _():
        to_right.start()

    @pl.when(me > 0)
    def _():
        to_left.start()

    @pl.when(me == 0)
    def _():
        low_kv[...] = jnp.zeros_like(low_kv)

    @pl.when(me == n_ep - 1)
    def _():
        high_kv[...] = jnp.zeros_like(high_kv)

    for k in far:
        start(net(k, 0))

    for q in range(n_pair):
        for side in range(2):
            owner = 2 * pair_up[q] + (core if side == 0 else 1 - core)
            rows = close_onehot if side == 0 else close_onehot[:cap]
            slots = jnp.dot(rows, normed_v[:, columns_of(owner, slice_width)], preferred_element_type=f32)
            rows_in[owner, 0] = pack(slots[:cap]).astype(bf16)
            if side == 0:
                for place, k in enumerate(close[1:]):
                    place = (place + 1) * cap
                    packed[q, k] = pack(slots[place : place + cap]).astype(bf16)
        for k in close[1:]:
            start(net(k, q))

    loads[12].wait()
    loads[7].wait()
    query = [
        turn(query_v[:, pl.ds(column, LANES)]) for column in range(0, query_v.shape[1], LANES)
    ]
    span = row_count + 2 * WINDOW
    local = lax.broadcasted_iota(jnp.int32, (row_count, span), 0)
    other = lax.broadcasted_iota(jnp.int32, (row_count, span), 1) - WINDOW
    position = me * row_count + other
    allowed = (
        (jnp.abs(local - other) <= WINDOW) & (position >= 0) & (position < row_count * n_ep)
    )

    @pl.when(me > 0)
    def _():
        to_right.wait_recv()

    @pl.when(me < n_ep - 1)
    def _():
        to_left.wait_recv()

    both = jnp.concatenate([low_kv[...], own_kv[...], high_kv[...]], axis=0).astype(f32)
    both_roll = pltpu.roll(both, head_dim, 1)
    low_span = lax.broadcasted_iota(jnp.int32, (span, LANES), 1) < head_dim
    keys = jnp.where(low_span, both, both_roll).astype(bf16)
    values = jnp.where(low_span, both_roll, both).astype(bf16)
    blocks = []
    for head in range(local_heads):
        mine = low_lane if head % 2 == 0 else jnp.logical_not(low_lane)
        head_query = jnp.where(mine, query[head // 2], 0.0).astype(bf16)
        scores = lax.dot_general(
            head_query, keys, (((1,), (1,)), ((), ())), preferred_element_type=f32
        ) * head_dim ** (-0.5)
        scores = jnp.where(allowed, scores, MASK_VALUE)
        sink = sink_v[:, head : head + 1]
        largest = jnp.maximum(jnp.max(scores, axis=-1, keepdims=True), sink)
        weights = jnp.exp(scores - largest)
        denominator = jnp.sum(weights, axis=-1, keepdims=True) + jnp.exp(sink - largest)
        probability = (weights * (1.0 / denominator)).astype(bf16)
        result = jnp.dot(probability, values, preferred_element_type=f32)
        if head % 2 == 0:
            blocks.append(result)
        else:
            blocks[-1] = jnp.where(low_lane, blocks[-1], result)
    attended = jnp.concatenate(blocks, axis=1).astype(bf16)[:, : local_heads * head_dim]
    loads[8].wait()
    partial_sum = jnp.dot(attended, out_w[...], preferred_element_type=f32)
    mix_send[...] = partial_sum.reshape(mix_send.shape).astype(bf16)

    def mix_own(p):
        return 2 * pair_up[p] + (core if p == 0 else 1 - core)

    def mix_other(p):
        return 2 * pair_up[p] + (1 - core if p == 0 else core)

    mix_pairs = [
        remote(mix_send.at[mix_other(p)], mix_sib.at[p],
               send_sem.at[4], mix_sib_recv_sem.at[p], me, sibling)
        for p in range(n_pair)
    ]
    for p in list(range(1, n_pair)) + [0]:
        start(mix_pairs[p])

    loads[1].wait()
    blocked = halves * cap
    number = lax.broadcasted_iota(jnp.int32, (blocked, row_count), 0)
    slot_of = number
    left = number >= 0
    if tail:
        in_main = number < 2 * main
        slot_of = jnp.where(
            in_main,
            jnp.where(number < main, number, number - main),
            jnp.where(number < 2 * main + tail, number - main, number - main - tail),
        )
        left = (number < main) | (jnp.logical_not(in_main) & (number < 2 * main + tail))
    for k in range(n_ep):
        placed = jnp.zeros((blocked, row_count), f32)
        for j in range(TOP):
            chosen = jnp.where(routes[j] == experts_of[k], rank[j], -1) == slot_of
            placed = jnp.where(chosen, route_weight_v[j : j + 1, :], placed)
        combine_left[pl.ds(k * blocked, blocked)] = jnp.where(left, placed, 0.0).astype(bf16)
        if tail:
            combine_right[pl.ds(k * blocked, blocked)] = jnp.where(left, 0.0, placed).astype(bf16)

    def group_of(k):
        return [number for number, group in enumerate(groups) if k in group][0]

    def near_forward(k, q):
        owner = 2 * pair_up[q] + 1 - core
        return remote(rows_in.at[owner, k], rows_in.at[owner, k],
                      send_sem.at[2], near_recv_sem.at[group_of(k)], me, sibling)

    def far_forward(k, p):
        owner = 2 * pair + 1 - core
        return remote(rows_in.at[owner, k], rows_in.at[owner, k],
                      send_sem.at[3], far_recv_sem.at[p, k - half_count], me, 2 * pair_up[p] + 1 - core)

    def far_relay(k, p):
        owner = 2 * pair_down[p] + core
        return remote(rows_in.at[owner, k], rows_in.at[owner, k],
                      send_sem.at[2], near_recv_sem.at[group_of(k)], me, sibling)

    def forward(group):
        for k in group:
            if k == 0:
                continue
            if k >= half_count:
                net(k, 0).wait_recv()
                for p in range(1, n_pair):
                    start(far_forward(k, p))
                start(near_forward(k, 0))
                continue
            arrived(rows_in.at[pl.ds(0, n_pair), k], net_recv_sem.at[k])
            for q in range(n_pair):
                start(near_forward(k, q))

    def relay(group):
        for k in group:
            if k < half_count:
                continue
            for p in range(1, n_pair):
                far_forward(k, p).wait_recv()
                start(far_relay(k, p))

    def gather(group):
        count = len(group) - (0 in group)
        arrived(rows_in.at[pl.ds(0, n_pair), pl.ds(0, count)], near_recv_sem.at[group_of(group[0])])
        for owner in range(n_tp):
            for half in range(halves):
                columns = pl.ds(owner * slice_width + half * piece, piece)
                for place, k in enumerate(group):
                    gathered[pl.ds(place * main, main), columns] = (
                        rows_in[owner, k, pl.ds(half * main, main), :]
                    )
                if tail:
                    ends = [
                        rows_in[owner, k, pl.ds(2 * main, 2 * tail), :].astype(f32)[
                            half * tail : (half + 1) * tail
                        ]
                        for k in group
                    ]
                    gathered[pl.ds(len(group) * main, len(group) * tail), columns] = (
                        jnp.concatenate(ends, axis=0).astype(bf16)
                    )

    hidden_width = gate_w.shape[1]
    tile = min(hidden_width, 512)

    def expand(group):
        rows = len(group) * cap

        for number in range(hidden_width // tile):
            columns = pl.ds(number * tile, tile)
            gate_act = jnp.dot(gathered[:rows], gate_w[:, columns], preferred_element_type=f32)
            up_act = jnp.dot(gathered[:rows], up_w[:, columns], preferred_element_type=f32)
            hidden[:rows, columns] = (gate_act / (1.0 + jnp.exp(-gate_act)) * up_act).astype(bf16)

    def down_slice(group, owner):
        rows = len(group) * cap
        result = jnp.dot(
            hidden[:rows], down_w[:, columns_of(owner, slice_width)], preferred_element_type=f32
        )
        count = len(group)
        for place, k in enumerate(group):
            values = result[place * main : (place + 1) * main]
            if tail:
                last = count * main + place * tail
                values = jnp.concatenate([values, result[last : last + tail]], axis=0)
            yield k, pack(values)

    def batches(group):
        return [group[0] + start for start in range(0, len(group), 2)]

    def sib_copy(k, p):
        both = pl.ds(k, 2)
        return remote(sib_send.at[p, both], sib_recv.at[p, both],
                      send_sem.at[5], sib_recv_sem.at[p, k // 2], me, sibling)

    def cross_copy(k, p):
        both = pl.ds(k, 2)
        return remote(cross_send.at[p, both], cross_recv.at[p, both],
                      send_sem.at[6], cross_recv_sem.at[p, k // 2], me, 2 * pair_up[p] + 1 - core)

    def return_copy(k):
        return remote(final_send.at[k], returned.at[k],
                      send_sem.at[7], final_recv_sem.at[0], experts_of[k], sibling)

    def contract(group):
        for p in list(range(1, n_pair)) + [0]:
            given = 2 * pair_up[p] + (core if p == 0 else 1 - core)
            kept = 2 * pair_up[p] + (1 - core if p == 0 else core)
            for k, values in down_slice(group, given):
                sib_send[p, k] = values.astype(bf16)
            for k in batches(group):
                start(sib_copy(k, p))
            for k, values in down_slice(group, kept):
                own_acc[p, k] = values

    def cross(group):
        for first in batches(group):
            for p in range(1, n_pair):
                sib_copy(first, p).wait_recv()
                for k in (first, first + 1):
                    cross_send[p, k] = (own_acc[p, k] + sib_recv[p, k].astype(f32)).astype(bf16)
                start(cross_copy(first, p))

    def finish(group):
        for first in batches(group):
            sib_copy(first, 0).wait_recv()
            for p in range(1, n_pair):
                cross_copy(first, p).wait_recv()
            for k in (first, first + 1):
                total = own_acc[0, k] + sib_recv[0, k].astype(f32)
                for p in range(1, n_pair):
                    total += cross_recv[p, k].astype(f32)
                final_send[k] = total.astype(bf16)
                start(return_copy(k))

    def mix_forward():
        for p in range(1, n_pair):
            mix_pairs[p].wait_recv()
            mix_cross[p] = (
                mix_send[mix_own(p)].astype(f32) + mix_sib[p].astype(f32)
            ).astype(bf16)
            start(mix_copy(p))

    def mix_copy(p):
        return remote(mix_cross.at[p], mix_recv.at[p],
                      send_sem.at[8], mix_recv_sem.at[p], me, 2 * pair_up[p] + 1 - core)

    def mix_finish():
        mix_pairs[0].wait_recv()
        mixed = mix_send[mix_own(0)].astype(f32) + mix_sib[0].astype(f32)
        for p in range(1, n_pair):
            mix_copy(p).wait_recv()
            mixed += mix_recv[p].astype(f32)
        mixer_ref[...] = mixed.astype(mixer_ref.dtype)

    first, second, last = groups
    forward(first)
    forward(second)
    mix_forward()
    relay(first)
    forward(last)
    loads[9].wait()
    loads[10].wait()
    gather(first)
    expand(first)
    relay(second)
    loads[11].wait()
    contract(first)
    gather(second)
    cross(first)
    expand(second)
    contract(second)
    gather(last)
    cross(second)
    expand(last)
    finish(first)
    contract(last)
    finish(second)
    cross(last)
    mix_finish()
    finish(last)

    arrived(returned, final_recv_sem.at[0])
    blocks = returned[...].reshape(n_ep * blocked, piece)

    def combined(weights_ref):
        return lax.dot_general(
            weights_ref[...], blocks, (((0,), (0,)), ((), ())), preferred_element_type=f32
        )

    expert_ref[:, :piece] = combined(combine_left).astype(expert_ref.dtype)
    if tail:
        expert_ref[:, piece:] = combined(combine_right).astype(expert_ref.dtype)

    @pl.when(me < n_ep - 1)
    def _():
        to_right.wait_send()

    @pl.when(me > 0)
    def _():
        to_left.wait_send()

    far_count = n_ep - half_count
    arrived(packed.at[0, pl.ds(0, far_count)], send_sem.at[0])
    arrived(packed.at[:, pl.ds(0, half_count - 1)], send_sem.at[1])
    arrived(rows_in.at[pl.ds(0, n_pair), pl.ds(0, n_ep - 1)], send_sem.at[2])
    if n_pair > 1:
        arrived(rows_in.at[pl.ds(0, n_pair - 1), pl.ds(0, far_count)], send_sem.at[3])
    arrived(mix_sib, send_sem.at[4])
    if n_pair > 1:
        arrived(mix_cross.at[pl.ds(0, n_pair - 1)], send_sem.at[8])
    arrived(sib_send, send_sem.at[5])
    if n_pair > 1:
        arrived(cross_send.at[pl.ds(0, n_pair - 1)], send_sem.at[6])
    arrived(final_send, send_sem.at[7])


def on_device(
    queries,
    key_states,
    value_states,
    sink_logit,
    out_weight,
    expert_input,
    norm_gain,
    routes,
    route_weight,
    gate_weight,
    up_weight,
    down_weight,
):
    n_ep = lax.axis_size("ep")
    n_tp = lax.axis_size("tp")
    row_count, width = expert_input.shape
    local_heads = queries.shape[1] // HEAD_DIM
    capacity = row_count * TOP * 5 // (4 * n_ep)
    main, tail = capacity // 16 * 16, 0
    if 0 < capacity - main <= 8 and width // n_tp >= 2 * LANES and main:
        tail = 8
    elif capacity > main:
        main += 16
    halves = 2 if tail else 1
    slice_width = width // n_tp
    piece = slice_width // halves
    blocked = halves * (main + tail)
    hidden_width = gate_weight.shape[2]
    mix_rows = row_count // n_tp
    n_pair = n_tp // 2
    group_rows = n_ep // 2 * (main + tail)
    if queries.shape[1] % LANES:
        queries = jnp.pad(queries, ((0, 0), (0, LANES - queries.shape[1] % LANES)))
    table = jnp.asarray(angle_table(row_count, n_ep))
    vmem = pl.BlockSpec(memory_space=pltpu.VMEM)
    hbm = pl.BlockSpec(memory_space=pltpu.HBM)
    bf16, f32 = jnp.bfloat16, jnp.float32
    dma = pltpu.SemaphoreType.DMA
    traveling = (blocked, piece)
    mixer_out, expert_out = pl.pallas_call(
        functools.partial(fused_kernel, (n_ep, n_tp, main, tail)),
        out_shape=(
            jax.ShapeDtypeStruct((mix_rows, width), bf16),
            jax.ShapeDtypeStruct((row_count, slice_width), bf16),
        ),
        in_specs=[hbm] * 13,
        out_specs=(vmem, vmem),
        scratch_shapes=[
            pltpu.VMEM(queries.shape, bf16),
            pltpu.VMEM((row_count, LANES), bf16),
            pltpu.VMEM((row_count, LANES), bf16),
            pltpu.VMEM(table.shape, f32),
            pltpu.VMEM((1, local_heads), f32),
            pltpu.VMEM(expert_input.shape, bf16),
            pltpu.VMEM((1, width), f32),
            pltpu.VMEM((TOP, row_count), jnp.int32),
            pltpu.VMEM((TOP, row_count), f32),
            pltpu.VMEM(out_weight.shape, bf16),
            pltpu.VMEM(gate_weight.shape[1:], bf16),
            pltpu.VMEM(up_weight.shape[1:], bf16),
            pltpu.VMEM(down_weight.shape[1:], bf16),
            pltpu.VMEM(expert_input.shape, bf16),
            pltpu.VMEM((row_count, LANES), bf16),
            pltpu.VMEM((row_count, LANES), bf16),
            pltpu.VMEM((WINDOW, LANES), bf16),
            pltpu.VMEM((WINDOW, LANES), bf16),
            pltpu.VMEM((n_pair, n_ep) + traveling, bf16),
            pltpu.VMEM((n_tp, n_ep) + traveling, bf16),
            pltpu.VMEM((group_rows, width), bf16),
            pltpu.VMEM((group_rows, hidden_width), bf16),
            pltpu.VMEM((n_tp, mix_rows, width), bf16),
            pltpu.VMEM((n_pair, mix_rows, width), bf16),
            pltpu.VMEM((n_pair, mix_rows, width), bf16),
            pltpu.VMEM((n_pair, mix_rows, width), bf16),
            pltpu.VMEM((n_pair, n_ep) + traveling, bf16),
            pltpu.VMEM((n_pair, n_ep) + traveling, bf16),
            pltpu.VMEM((n_pair, n_ep) + traveling, f32),
            pltpu.VMEM((n_pair, n_ep) + traveling, bf16),
            pltpu.VMEM((n_pair, n_ep) + traveling, bf16),
            pltpu.VMEM((n_ep,) + traveling, bf16),
            pltpu.VMEM((n_ep,) + traveling, bf16),
            pltpu.VMEM((n_ep * blocked, row_count), bf16),
            pltpu.VMEM((n_ep * blocked, row_count), bf16),
            dma((13,)),
            dma((2,)),
            dma((2,)),
            dma((9,)),
            dma((n_ep,)),
            dma((n_pair, n_ep // 2)),
            dma((3,)),
            dma((n_pair,)),
            dma((n_pair,)),
            dma((n_pair, n_ep // 2)),
            dma((n_pair, n_ep // 2)),
            dma((1,)),
        ],
        compiler_params=pltpu.CompilerParams(
            collective_id=0, has_side_effects=True, vmem_limit_bytes=60 * 1024 * 1024
        ),
    )(
        queries,
        key_states,
        value_states,
        table,
        sink_logit[None, :],
        expert_input,
        norm_gain[None, :],
        routes.T,
        route_weight.T,
        out_weight,
        gate_weight,
        up_weight,
        down_weight,
    )
    return mixer_out, expert_out


def solution(mesh):
    in_specs = (
        P("ep", "tp"),
        P("ep", None),
        P("ep", None),
        P("tp"),
        P("tp", None),
        P("ep", None),
        P(),
        P("ep", None),
        P("ep", None),
        P("ep", None, "tp"),
        P("ep", None, "tp"),
        P("ep", "tp", None),
    )
    out_specs = (P(("ep", "tp"), None), P("ep", "tp"))
    return jax.shard_map(
        on_device, mesh=mesh, in_specs=in_specs, out_specs=out_specs, check_vma=False
    )
```

time: 55.6 us -> 43 us (0.77)
  Pallas kernels: 47 us -> 39.1 us
  other arithmetic: 5.46 us -> 0 us
  local copies, waits for them, and re-layouts: 2.08 us -> 3.14 us
    pallas_call x1, Pallas kernels: 47 us -> 39.1 us  [on_device(): pl.pallas_call(functools.partial(fused_kernel, (n_ep, n_tp, main, tail)),...]
    convert_element_type x4 -> x0, other arithmetic: 3.26 us -> none  [the longest x2 3.24 us: on_device(): return (mixer_out.astype(bf16), expert_out.astype(bf16))]
    unnamed x2, local copies, waits for them, and re-layouts: 1.08 us -> 3.14 us
    another operation x1 -> x0, local copies, waits for them, and re-layouts: 0.87 us -> none  [on_device(): jnp.stack([turned_key, own_value])]
    another operation x2 -> x0, other arithmetic: 0.8 us -> none  [the longest x1 0.71 us: on_device(): jnp.stack([turned_key, own_value])]
    transpose x1 -> x0, other arithmetic: 0.77 us -> none  [on_device(): turned_query.transpose(1, 0, 2)]
where the time goes in v1:
time: 43 us; the launch traced here: 42.9 us
  Pallas kernels  39.1 us (91%)
  local copies, waits for them, and re-layouts  3.14 us (7%)
  between operations  0.64 us (1%)
    pallas_call x1, Pallas kernels, on_device(): pl.pallas_call(functools.partial(fused_kernel, (n_ep, n_tp, main, tail)),...  39.1 us
    unnamed x2, local copies, waits for them, and re-layouts  3.14 us

profile of v1, /device:TPU:0, one launch (start us, length us, event | category | flops | bytes accessed | tf_op | source)
XLA Modules:
  0.0 42.9 jit_solution(6325962650573303108)
XLA Ops:
  0.6 39.1 %shard_map.140 = (bf16[32,2048]{1,0:T(8,128)(2,1)}, bf16[128,512]{1,0:T(8,128)(2,1)}) custom-call(bf16[128,256]{1,0:T(8,128)(2,1)} %query_hbm.1, bf16[128,256]{1,0:T(8,128)(2,1)} %key_hbm.1, bf16[128,256]{1,0:T(8,128)(2,1)} %value_hbm.1, f32[272,128]{1,0:T(8,128)} %constant.2.clone.table_hbm, f32[1,4]{1,0:T(1,128)} %bitcast.7, bf16[128,2048]{1,0:T(8,128)(2,1)} %input_hbm.1, ...), custom_call_target="tpu_custom_call" | custom-call | tf_op jit(solution)/shard_map/pallas_call | solution.py:663
  39.7 1.6 %copy.17 = bf16[32,2048]{1,0:T(8,128)(2,1)} copy(bf16[32,2048]{1,0:T(8,128)(2,1)} %get-tuple-element.4) | data formatting | bytes 262144
  41.3 1.6 %copy.18 = bf16[128,512]{1,0:T(8,128)(2,1)} copy(bf16[128,512]{1,0:T(8,128)(2,1)} %get-tuple-element.5) | data formatting | bytes 262144

commit v2 on v1

--- a/solution.py
+++ b/solution.py
@@ -130,13 +130,25 @@
     head_dim = HEAD_DIM
     local_heads = sink_v.shape[1]
     half_count = n_ep // 2
-    near = list(range(half_count))
-    groups = [
-        list(range(3 * n_ep // 4, n_ep)),
-        list(range(half_count, 3 * n_ep // 4)),
-        near,
+    quarter = n_ep // 4
+    experts_of = [partner(me, k) for k in range(n_ep)]
+    middle = lax.rem(me // half_count + me // quarter, 2)
+    bases = [half_count + quarter * (1 - middle), half_count + quarter * middle]
+    far_experts = [
+        [
+            experts_of[half_count + quarter * place + i]
+            + middle * (experts_of[half_count + quarter * (1 - place) + i]
+                        - experts_of[half_count + quarter * place + i])
+            for i in range(quarter)
+        ]
+        for place in (1, 0)
     ]
-    experts_of = [partner(me, k) for k in range(n_ep)]
+    far_batches = [(bases[place], far_experts[place]) for place in range(2)]
+    near_batches = [
+        (0, experts_of[:quarter]),
+        (quarter, experts_of[quarter:half_count]),
+    ]
+    groups = [(far_batches[place], near_batches[place]) for place in range(2)]
     pair_up = [lax.rem(pair + p, n_pair) for p in range(n_pair)]
     pair_down = [lax.rem(pair + n_pair - p, n_pair) for p in range(n_pair)]
 
@@ -223,9 +235,8 @@
         parts = [values[:main, :piece], values[:main, piece:], values[main:, :piece], values[main:, piece:]]
         return jnp.concatenate(parts, axis=0)
 
-    order = [k for group in groups for k in group]
-    far = [k for k in order if k >= half_count]
-    close = [k for k in order if k < half_count]
+    far = list(range(half_count, n_ep))
+    close = list(range(half_count))
     for number in range(4, 7):
         loads[number].wait()
     lane = lax.broadcasted_iota(jnp.int32, (row_count, LANES), 1)
@@ -282,10 +293,10 @@
 
     pl.semaphore_wait(barrier, n_ep + n_tp - 2)
 
-    def net(k, q):
+    def net(k, expert, q, sem):
         owner = 2 * pair_up[q] + core
         return remote(packed.at[q, k], rows_in.at[owner, k],
-                      send_sem.at[0 if k >= half_count else 1], net_recv_sem.at[k], experts_of[k], sibling)
+                      send_sem.at[sem], net_recv_sem.at[k], expert, sibling)
 
     @pl.when(me < n_ep - 1)
     def _():
@@ -303,8 +314,9 @@
     def _():
         high_kv[...] = jnp.zeros_like(high_kv)
 
-    for k in far:
-        start(net(k, 0))
+    for base, experts in far_batches:
+        for i, expert in enumerate(experts):
+            start(net(base + i, expert, 0, 0))
 
     for q in range(n_pair):
         for side in range(2):
@@ -316,8 +328,10 @@
                 for place, k in enumerate(close[1:]):
                     place = (place + 1) * cap
                     packed[q, k] = pack(slots[place : place + cap]).astype(bf16)
-        for k in close[1:]:
-            start(net(k, q))
+
+    for k in close[1:]:
+        for q in range(n_pair):
+            start(net(k, experts_of[k], q, 1))
 
     loads[12].wait()
     loads[7].wait()
@@ -404,53 +418,55 @@
         if tail:
             combine_right[pl.ds(k * blocked, blocked)] = jnp.where(left, 0.0, placed).astype(bf16)
 
-    def group_of(k):
-        return [number for number, group in enumerate(groups) if k in group][0]
-
-    def near_forward(k, q):
+    def near_forward(k, q, sem):
         owner = 2 * pair_up[q] + 1 - core
         return remote(rows_in.at[owner, k], rows_in.at[owner, k],
-                      send_sem.at[2], near_recv_sem.at[group_of(k)], me, sibling)
+                      send_sem.at[2], near_recv_sem.at[sem], me, sibling)
 
     def far_forward(k, p):
         owner = 2 * pair + 1 - core
         return remote(rows_in.at[owner, k], rows_in.at[owner, k],
                       send_sem.at[3], far_recv_sem.at[p, k - half_count], me, 2 * pair_up[p] + 1 - core)
 
-    def far_relay(k, p):
+    def far_relay(k, p, sem):
         owner = 2 * pair_down[p] + core
         return remote(rows_in.at[owner, k], rows_in.at[owner, k],
-                      send_sem.at[2], near_recv_sem.at[group_of(k)], me, sibling)
-
-    def forward(group):
-        for k in group:
-            if k == 0:
-                continue
-            if k >= half_count:
-                net(k, 0).wait_recv()
-                for p in range(1, n_pair):
-                    start(far_forward(k, p))
-                start(near_forward(k, 0))
-                continue
+                      send_sem.at[2], near_recv_sem.at[sem], me, sibling)
+
+    def forward_far(number):
+        base, experts = far_batches[number]
+        for i, expert in enumerate(experts):
+            net(base + i, expert, 0, 0).wait_recv()
+            for p in range(1, n_pair):
+                start(far_forward(base + i, p))
+            start(near_forward(base + i, 0, number))
+
+    def relay_far(number):
+        base, experts = far_batches[number]
+        for i in range(len(experts)):
+            for p in range(1, n_pair):
+                far_forward(base + i, p).wait_recv()
+                start(far_relay(base + i, p, number))
+
+    def forward_near(number):
+        base, experts = near_batches[number]
+        for k in range(max(base, 1), base + len(experts)):
             arrived(rows_in.at[pl.ds(0, n_pair), k], net_recv_sem.at[k])
             for q in range(n_pair):
-                start(near_forward(k, q))
-
-    def relay(group):
-        for k in group:
-            if k < half_count:
-                continue
-            for p in range(1, n_pair):
-                far_forward(k, p).wait_recv()
-                start(far_relay(k, p))
-
-    def gather(group):
-        count = len(group) - (0 in group)
-        arrived(rows_in.at[pl.ds(0, n_pair), pl.ds(0, count)], near_recv_sem.at[group_of(group[0])])
+                start(near_forward(k, q, 2 + number))
+
+    def gather(number):
+        slots = []
+        for kind, (base, experts) in enumerate(groups[number]):
+            count = len(experts)
+            slots += [base + i for i in range(count)]
+            if kind == 1 and number == 0:
+                count -= 1
+            arrived(rows_in.at[pl.ds(0, n_pair), pl.ds(0, count)], near_recv_sem.at[2 * kind + number])
         for owner in range(n_tp):
             for half in range(halves):
                 columns = pl.ds(owner * slice_width + half * piece, piece)
-                for place, k in enumerate(group):
+                for place, k in enumerate(slots):
                     gathered[pl.ds(place * main, main), columns] = (
                         rows_in[owner, k, pl.ds(half * main, main), :]
                     )
@@ -459,84 +475,77 @@
                         rows_in[owner, k, pl.ds(2 * main, 2 * tail), :].astype(f32)[
                             half * tail : (half + 1) * tail
                         ]
-                        for k in group
+                        for k in slots
                     ]
-                    gathered[pl.ds(len(group) * main, len(group) * tail), columns] = (
+                    gathered[pl.ds(len(slots) * main, len(slots) * tail), columns] = (
                         jnp.concatenate(ends, axis=0).astype(bf16)
                     )
 
     hidden_width = gate_w.shape[1]
     tile = min(hidden_width, 512)
 
-    def expand(group):
-        rows = len(group) * cap
-
+    rows = half_count * cap
+
+    def expand():
         for number in range(hidden_width // tile):
             columns = pl.ds(number * tile, tile)
-            gate_act = jnp.dot(gathered[:rows], gate_w[:, columns], preferred_element_type=f32)
-            up_act = jnp.dot(gathered[:rows], up_w[:, columns], preferred_element_type=f32)
-            hidden[:rows, columns] = (gate_act / (1.0 + jnp.exp(-gate_act)) * up_act).astype(bf16)
-
-    def down_slice(group, owner):
-        rows = len(group) * cap
+            gate_act = jnp.dot(gathered[...], gate_w[:, columns], preferred_element_type=f32)
+            up_act = jnp.dot(gathered[...], up_w[:, columns], preferred_element_type=f32)
+            hidden[:, columns] = (gate_act / (1.0 + jnp.exp(-gate_act)) * up_act).astype(bf16)
+
+    def down_slice(number, owner):
         result = jnp.dot(
-            hidden[:rows], down_w[:, columns_of(owner, slice_width)], preferred_element_type=f32
+            hidden[...], down_w[:, columns_of(owner, slice_width)], preferred_element_type=f32
         )
-        count = len(group)
-        for place, k in enumerate(group):
+        slots = [base + i for base, experts in groups[number] for i in range(len(experts))]
+        for place, k in enumerate(slots):
             values = result[place * main : (place + 1) * main]
             if tail:
-                last = count * main + place * tail
+                last = half_count * main + place * tail
                 values = jnp.concatenate([values, result[last : last + tail]], axis=0)
             yield k, pack(values)
 
-    def batches(group):
-        return [group[0] + start for start in range(0, len(group), 2)]
-
-    def sib_copy(k, p):
-        both = pl.ds(k, 2)
-        return remote(sib_send.at[p, both], sib_recv.at[p, both],
-                      send_sem.at[5], sib_recv_sem.at[p, k // 2], me, sibling)
+    def sib_copy(base, p):
+        batch = pl.ds(base, quarter)
+        return remote(sib_send.at[p, batch], sib_recv.at[p, batch],
+                      send_sem.at[5], sib_recv_sem.at[p, base // quarter], me, sibling)
 
     def cross_copy(k, p):
-        both = pl.ds(k, 2)
-        return remote(cross_send.at[p, both], cross_recv.at[p, both],
-                      send_sem.at[6], cross_recv_sem.at[p, k // 2], me, 2 * pair_up[p] + 1 - core)
-
-    def return_copy(k):
-        return remote(final_send.at[k], returned.at[k],
-                      send_sem.at[7], final_recv_sem.at[0], experts_of[k], sibling)
-
-    def contract(group):
+        return remote(cross_send.at[p, k], cross_recv.at[p, k],
+                      send_sem.at[6], cross_recv_sem.at[p - 1, k], me, 2 * pair_up[p] + 1 - core)
+
+    def contract(number):
         for p in list(range(1, n_pair)) + [0]:
             given = 2 * pair_up[p] + (core if p == 0 else 1 - core)
             kept = 2 * pair_up[p] + (1 - core if p == 0 else core)
-            for k, values in down_slice(group, given):
+            for k, values in down_slice(number, given):
                 sib_send[p, k] = values.astype(bf16)
-            for k in batches(group):
-                start(sib_copy(k, p))
-            for k, values in down_slice(group, kept):
+            for base, _ in groups[number]:
+                start(sib_copy(base, p))
+            for k, values in down_slice(number, kept):
                 own_acc[p, k] = values
 
-    def cross(group):
-        for first in batches(group):
+    def cross(batch):
+        base = batch[0]
+        for p in range(1, n_pair):
+            sib_copy(base, p).wait_recv()
+            for i in range(quarter):
+                k = base + i
+                cross_send[p, k] = (own_acc[p, k] + sib_recv[p, k].astype(f32)).astype(bf16)
+                start(cross_copy(k, p))
+
+    def finish(batch):
+        base, experts = batch
+        sib_copy(base, 0).wait_recv()
+        for i, expert in enumerate(experts):
+            k = base + i
+            total = own_acc[0, k] + sib_recv[0, k].astype(f32)
             for p in range(1, n_pair):
-                sib_copy(first, p).wait_recv()
-                for k in (first, first + 1):
-                    cross_send[p, k] = (own_acc[p, k] + sib_recv[p, k].astype(f32)).astype(bf16)
-                start(cross_copy(first, p))
-
-    def finish(group):
-        for first in batches(group):
-            sib_copy(first, 0).wait_recv()
-            for p in range(1, n_pair):
-                cross_copy(first, p).wait_recv()
-            for k in (first, first + 1):
-                total = own_acc[0, k] + sib_recv[0, k].astype(f32)
-                for p in range(1, n_pair):
-                    total += cross_recv[p, k].astype(f32)
-                final_send[k] = total.astype(bf16)
-                start(return_copy(k))
+                cross_copy(k, p).wait_recv()
+                total += cross_recv[p, k].astype(f32)
+            final_send[k] = total.astype(bf16)
+            start(remote(final_send.at[k], returned.at[k],
+                         send_sem.at[7], final_recv_sem.at[0], expert, sibling))
 
     def mix_forward():
         for p in range(1, n_pair):
@@ -558,32 +567,31 @@
             mixed += mix_recv[p].astype(f32)
         mixer_ref[...] = mixed.astype(mixer_ref.dtype)
 
-    first, second, last = groups
-    forward(first)
-    forward(second)
+    forward_far(0)
+    forward_near(0)
+    forward_far(1)
+    relay_far(0)
     mix_forward()
-    relay(first)
-    forward(last)
     loads[9].wait()
     loads[10].wait()
-    gather(first)
-    expand(first)
-    relay(second)
+    gather(0)
+    expand()
+    relay_far(1)
+    forward_near(1)
     loads[11].wait()
-    contract(first)
-    gather(second)
-    cross(first)
-    expand(second)
-    contract(second)
-    gather(last)
-    cross(second)
-    expand(last)
-    finish(first)
-    contract(last)
-    finish(second)
-    cross(last)
+    contract(0)
+    cross(far_batches[0])
+    gather(1)
+    cross(near_batches[0])
+    expand()
+    contract(1)
+    cross(far_batches[1])
+    finish(far_batches[0])
+    cross(near_batches[1])
+    finish(near_batches[0])
+    finish(far_batches[1])
     mix_finish()
-    finish(last)
+    finish(near_batches[1])
 
     arrived(returned, final_recv_sem.at[0])
     blocks = returned[...].reshape(n_ep * blocked, piece)
@@ -660,6 +668,21 @@
     bf16, f32 = jnp.bfloat16, jnp.float32
     dma = pltpu.SemaphoreType.DMA
     traveling = (blocked, piece)
+    operands = (
+        queries,
+        key_states,
+        value_states,
+        table,
+        sink_logit[None, :],
+        expert_input,
+        norm_gain[None, :],
+        routes.T,
+        route_weight.T,
+        out_weight,
+        gate_weight,
+        up_weight,
+        down_weight,
+    )
     mixer_out, expert_out = pl.pallas_call(
         functools.partial(fused_kernel, (n_ep, n_tp, main, tail)),
         out_shape=(
@@ -710,31 +733,20 @@
             dma((9,)),
             dma((n_ep,)),
             dma((n_pair, n_ep // 2)),
-            dma((3,)),
+            dma((4,)),
             dma((n_pair,)),
             dma((n_pair,)),
-            dma((n_pair, n_ep // 2)),
-            dma((n_pair, n_ep // 2)),
+            dma((n_pair, 4)),
+            dma((n_pair - 1, n_ep)),
             dma((1,)),
         ],
         compiler_params=pltpu.CompilerParams(
-            collective_id=0, has_side_effects=True, vmem_limit_bytes=60 * 1024 * 1024
+            collective_id=0, has_side_effects=True, vmem_limit_bytes=50000 * 1024
         ),
-    )(
-        queries,
-        key_states,
-        value_states,
-        table,
-        sink_logit[None, :],
-        expert_input,
-        norm_gain[None, :],
-        routes.T,
-        route_weight.T,
-        out_weight,
-        gate_weight,
-        up_weight,
-        down_weight,
-    )
+    )(*[
+        pltpu.with_memory_space_constraint(operand, pltpu.HBM) if operand.size > 1 else operand
+        for operand in operands
+    ])
     return mixer_out, expert_out
 
 

time: 43 us -> 36.3 us (0.84)
  Pallas kernels: 39.1 us -> 34.2 us
  local copies, waits for them, and re-layouts: 3.14 us -> 1.31 us
    pallas_call x1, Pallas kernels: 39.1 us -> 34.2 us  [on_device(): pl.pallas_call(functools.partial(fused_kernel, (n_ep, n_tp, main, tail)),...]
    unnamed x2, local copies, waits for them, and re-layouts: 3.14 us -> 1.31 us
where the time goes in v2:
time: 36.3 us; the launch traced here: 36.2 us
  Pallas kernels  34.2 us (94%)
  local copies, waits for them, and re-layouts  1.31 us (4%)
  between operations  0.64 us (2%)
    pallas_call x1, Pallas kernels, on_device(): pl.pallas_call(functools.partial(fused_kernel, (n_ep, n_tp, main, tail)),...  34.2 us
    unnamed x2, local copies, waits for them, and re-layouts  1.31 us

profile of v2, /device:TPU:0, one launch (start us, length us, event | category | flops | bytes accessed | tf_op | source)
XLA Modules:
  0.0 36.2 jit_solution(15478297028459600265)
XLA Ops:
  0.6 34.2 %shard_map.140 = (bf16[32,2048]{1,0:T(8,128)(2,1)S(1)}, bf16[128,512]{1,0:T(8,128)(2,1)S(1)}) custom-call(bf16[128,256]{1,0:T(8,128)(2,1)} %query_hbm.1, bf16[128,256]{1,0:T(8,128)(2,1)} %key_hbm.1, bf16[128,256]{1,0:T(8,128)(2,1)} %value_hbm.1, f32[272,128]{1,0:T(8,128)} %constant.2.clone.table_hbm, f32[1,4]{1,0:T(1,128)} %bitcast.7, ...), custom_call_target="tpu_custom_call" | custom-call | tf_op jit(solution)/shard_map/pallas_call | solution.py:686
  34.9 0.7 %copy.17 = bf16[32,2048]{1,0:T(8,128)(2,1)} copy(bf16[32,2048]{1,0:T(8,128)(2,1)S(1)} %get-tuple-element.4) | data formatting | bytes 262144
  35.5 0.7 %copy.18 = bf16[128,512]{1,0:T(8,128)(2,1)} copy(bf16[128,512]{1,0:T(8,128)(2,1)S(1)} %get-tuple-element.5) | data formatting | bytes 262144

commit v3 on v2

--- a/solution.py
+++ b/solution.py
@@ -198,8 +198,8 @@
             barrier, inc=1, device_id=(me, lax.rem(my_tp + step, n_tp)),
             device_id_type=pl.DeviceIdType.MESH,
         )
-    for load in loads:
-        load.start()
+    for number in [0, 2, 3, 4, 5, 6, 7, 12, 1, 8, 9, 10, 11]:
+        loads[number].start()
 
     def start(copy):
         copy.start()
@@ -338,13 +338,32 @@
     query = [
         turn(query_v[:, pl.ds(column, LANES)]) for column in range(0, query_v.shape[1], LANES)
     ]
-    span = row_count + 2 * WINDOW
-    local = lax.broadcasted_iota(jnp.int32, (row_count, span), 0)
-    other = lax.broadcasted_iota(jnp.int32, (row_count, span), 1) - WINDOW
-    position = me * row_count + other
-    allowed = (
-        (jnp.abs(local - other) <= WINDOW) & (position >= 0) & (position < row_count * n_ep)
-    )
+    local = lax.broadcasted_iota(jnp.int32, (row_count, WINDOW), 0)
+    other = lax.broadcasted_iota(jnp.int32, (row_count, WINDOW), 1)
+
+    def split_heads(packed_rows):
+        both = packed_rows.astype(f32)
+        swapped = pltpu.roll(both, head_dim, 1)
+        low = lax.broadcasted_iota(jnp.int32, both.shape, 1) < head_dim
+        return jnp.where(low, both, swapped).astype(bf16), jnp.where(low, swapped, both).astype(bf16)
+
+    own_rows = jnp.abs(
+        lax.broadcasted_iota(jnp.int32, (row_count, row_count), 0)
+        - lax.broadcasted_iota(jnp.int32, (row_count, row_count), 1)
+    ) <= WINDOW
+    own_keys, own_values = split_heads(own_kv[...])
+    head_queries, own_scores = [], []
+
+    def score(head_query, keys, allowed):
+        scores = lax.dot_general(
+            head_query, keys, (((1,), (1,)), ((), ())), preferred_element_type=f32
+        ) * head_dim ** (-0.5)
+        return jnp.where(allowed, scores, MASK_VALUE)
+
+    for head in range(local_heads):
+        mine = low_lane if head % 2 == 0 else jnp.logical_not(low_lane)
+        head_queries.append(jnp.where(mine, query[head // 2], 0.0).astype(bf16))
+        own_scores.append(score(head_queries[head], own_keys, own_rows))
 
     @pl.when(me > 0)
     def _():
@@ -354,24 +373,30 @@
     def _():
         to_left.wait_recv()
 
-    both = jnp.concatenate([low_kv[...], own_kv[...], high_kv[...]], axis=0).astype(f32)
-    both_roll = pltpu.roll(both, head_dim, 1)
-    low_span = lax.broadcasted_iota(jnp.int32, (span, LANES), 1) < head_dim
-    keys = jnp.where(low_span, both, both_roll).astype(bf16)
-    values = jnp.where(low_span, both_roll, both).astype(bf16)
+    low_allowed = (local - (other - WINDOW) <= WINDOW) & (me > 0)
+    high_allowed = (row_count + other - local <= WINDOW) & (me < n_ep - 1)
+    low_keys, low_values = split_heads(low_kv[...])
+    high_keys, high_values = split_heads(high_kv[...])
+    values = jnp.concatenate([low_values, own_values, high_values], axis=0)
     blocks = []
     for head in range(local_heads):
-        mine = low_lane if head % 2 == 0 else jnp.logical_not(low_lane)
-        head_query = jnp.where(mine, query[head // 2], 0.0).astype(bf16)
-        scores = lax.dot_general(
-            head_query, keys, (((1,), (1,)), ((), ())), preferred_element_type=f32
-        ) * head_dim ** (-0.5)
-        scores = jnp.where(allowed, scores, MASK_VALUE)
+        parts = [
+            score(head_queries[head], low_keys, low_allowed),
+            own_scores[head],
+            score(head_queries[head], high_keys, high_allowed),
+        ]
         sink = sink_v[:, head : head + 1]
-        largest = jnp.maximum(jnp.max(scores, axis=-1, keepdims=True), sink)
-        weights = jnp.exp(scores - largest)
-        denominator = jnp.sum(weights, axis=-1, keepdims=True) + jnp.exp(sink - largest)
-        probability = (weights * (1.0 / denominator)).astype(bf16)
+        highest = [jnp.max(part, axis=-1, keepdims=True) for part in parts]
+        if row_count == WINDOW:
+            highest = [jnp.max(functools.reduce(jnp.maximum, parts), axis=-1, keepdims=True)]
+        largest = functools.reduce(jnp.maximum, highest + [sink])
+        weights = [jnp.exp(part - largest) for part in parts]
+        totals = [jnp.sum(weight, axis=-1, keepdims=True) for weight in weights]
+        if row_count == WINDOW:
+            totals = [jnp.sum(functools.reduce(jnp.add, weights), axis=-1, keepdims=True)]
+        denominator = functools.reduce(jnp.add, totals) + jnp.exp(sink - largest)
+        scale = 1.0 / denominator
+        probability = jnp.concatenate([(weight * scale).astype(bf16) for weight in weights], axis=1)
         result = jnp.dot(probability, values, preferred_element_type=f32)
         if head % 2 == 0:
             blocks.append(result)
@@ -426,7 +451,7 @@
     def far_forward(k, p):
         owner = 2 * pair + 1 - core
         return remote(rows_in.at[owner, k], rows_in.at[owner, k],
-                      send_sem.at[3], far_recv_sem.at[p, k - half_count], me, 2 * pair_up[p] + 1 - core)
+                      send_sem.at[3], far_recv_sem.at[p - 1, k - half_count], me, 2 * pair_up[p] + 1 - core)
 
     def far_relay(k, p, sem):
         owner = 2 * pair_down[p] + core
@@ -514,31 +539,34 @@
         return remote(cross_send.at[p, k], cross_recv.at[p, k],
                       send_sem.at[6], cross_recv_sem.at[p - 1, k], me, 2 * pair_up[p] + 1 - core)
 
-    def contract(number):
-        for p in list(range(1, n_pair)) + [0]:
-            given = 2 * pair_up[p] + (core if p == 0 else 1 - core)
-            kept = 2 * pair_up[p] + (1 - core if p == 0 else core)
-            for k, values in down_slice(number, given):
-                sib_send[p, k] = values.astype(bf16)
-            for base, _ in groups[number]:
-                start(sib_copy(base, p))
-            for k, values in down_slice(number, kept):
-                own_acc[p, k] = values
-
-    def cross(batch):
+    def give(number, p):
+        owner = 2 * pair_up[p] + (core if p == 0 else 1 - core)
+        for k, values in down_slice(number, owner):
+            sib_send[p, k] = values.astype(bf16)
+        for base, _ in groups[number]:
+            start(sib_copy(base, p))
+
+    def keep(number, p):
+        owner = 2 * pair_up[p] + (1 - core if p == 0 else core)
+        for k, values in down_slice(number, owner):
+            own_acc[p, k] = values
+
+    def cross(batch, places=range(quarter)):
         base = batch[0]
         for p in range(1, n_pair):
-            sib_copy(base, p).wait_recv()
-            for i in range(quarter):
+            for i in places:
                 k = base + i
                 cross_send[p, k] = (own_acc[p, k] + sib_recv[p, k].astype(f32)).astype(bf16)
                 start(cross_copy(k, p))
 
-    def finish(batch):
+    def met(batch, parts):
+        for p in parts:
+            sib_copy(batch[0], p).wait_recv()
+
+    def finish(batch, places=range(quarter)):
         base, experts = batch
-        sib_copy(base, 0).wait_recv()
-        for i, expert in enumerate(experts):
-            k = base + i
+        for i in places:
+            k, expert = base + i, experts[i]
             total = own_acc[0, k] + sib_recv[0, k].astype(f32)
             for p in range(1, n_pair):
                 cross_copy(k, p).wait_recv()
@@ -567,6 +595,7 @@
             mixed += mix_recv[p].astype(f32)
         mixer_ref[...] = mixed.astype(mixer_ref.dtype)
 
+    others, rest = range(1, n_pair), range(1, quarter)
     forward_far(0)
     forward_near(0)
     forward_far(1)
@@ -576,22 +605,41 @@
     loads[10].wait()
     gather(0)
     expand()
+    loads[11].wait()
+    for p in others:
+        give(0, p)
     relay_far(1)
     forward_near(1)
-    loads[11].wait()
-    contract(0)
+    for p in others:
+        keep(0, p)
+    give(0, 0)
+    met(far_batches[0], others)
     cross(far_batches[0])
+    keep(0, 0)
     gather(1)
-    cross(near_batches[0])
+    met(near_batches[0], others)
+    cross(near_batches[0], rest)
     expand()
-    contract(1)
+    for p in others:
+        give(1, p)
+        keep(1, p)
+    give(1, 0)
+    met(far_batches[1], others)
     cross(far_batches[1])
+    met(far_batches[0], [0])
     finish(far_batches[0])
+    keep(1, 0)
+    met(near_batches[1], others)
     cross(near_batches[1])
-    finish(near_batches[0])
+    cross(near_batches[0], [0])
+    met(near_batches[0], [0])
+    finish(near_batches[0], rest)
+    met(far_batches[1], [0])
     finish(far_batches[1])
     mix_finish()
+    met(near_batches[1], [0])
     finish(near_batches[1])
+    finish(near_batches[0], [0])
 
     arrived(returned, final_recv_sem.at[0])
     blocks = returned[...].reshape(n_ep * blocked, piece)
@@ -626,6 +674,17 @@
     if n_pair > 1:
         arrived(cross_send.at[pl.ds(0, n_pair - 1)], send_sem.at[6])
     arrived(final_send, send_sem.at[7])
+
+
+def write_kernel(mixer_in, expert_in, mixer_out, expert_out, sem):
+    copies = [
+        pltpu.make_async_copy(mixer_in, mixer_out, sem.at[0]),
+        pltpu.make_async_copy(expert_in, expert_out, sem.at[1]),
+    ]
+    for copy in copies:
+        copy.start()
+    for copy in copies:
+        copy.wait()
 
 
 def on_device(
@@ -732,7 +791,7 @@
             dma((2,)),
             dma((9,)),
             dma((n_ep,)),
-            dma((n_pair, n_ep // 2)),
+            dma((n_pair - 1, n_ep // 2)),
             dma((4,)),
             dma((n_pair,)),
             dma((n_pair,)),
@@ -747,7 +806,17 @@
         pltpu.with_memory_space_constraint(operand, pltpu.HBM) if operand.size > 1 else operand
         for operand in operands
     ])
-    return mixer_out, expert_out
+    return pl.pallas_call(
+        write_kernel,
+        out_shape=(
+            jax.ShapeDtypeStruct(mixer_out.shape, bf16),
+            jax.ShapeDtypeStruct(expert_out.shape, bf16),
+        ),
+        in_specs=[vmem] * 2,
+        out_specs=(hbm, hbm),
+        scratch_shapes=[dma((2,))],
+        compiler_params=pltpu.CompilerParams(vmem_limit_bytes=1024 * 1024),
+    )(*[pltpu.with_memory_space_constraint(x, pltpu.VMEM) for x in (mixer_out, expert_out)])
 
 
 def solution(mesh):

time: 36.3 us -> 35 us (0.964)
  local copies, waits for them, and re-layouts: 1.31 us -> 0 us
    unnamed x2 -> x0, local copies, waits for them, and re-layouts: 1.31 us -> none
    pallas_call x1, Pallas kernels: 34.2 us -> 33.5 us  [on_device(): pl.pallas_call(functools.partial(fused_kernel, (n_ep, n_tp, main, tail)),...]
    pallas_call x0 -> x1, Pallas kernels: none -> 0.72 us  [on_device(): pl.pallas_call(write_kernel, out_shape=(jax.ShapeDtypeStruct(mixer_out.sh...]
where the time goes in v3:
time: 35 us; the launch traced here: 34.9 us
  Pallas kernels  34.2 us (98%)
  between operations  0.64 us (2%)
    pallas_call x1, Pallas kernels, on_device(): pl.pallas_call(functools.partial(fused_kernel, (n_ep, n_tp, main, tail)),...  33.5 us
    pallas_call x1, Pallas kernels, on_device(): pl.pallas_call(write_kernel, out_shape=(jax.ShapeDtypeStruct(mixer_out.sh...  0.72 us

profile of v3, /device:TPU:0, one launch (start us, length us, event | category | flops | bytes accessed | tf_op | source)
XLA Modules:
  0.0 34.9 jit_solution(10051125622561672455)
XLA Ops:
  0.6 33.5 %shard_map.140 = (bf16[32,2048]{1,0:T(8,128)(2,1)S(1)}, bf16[128,512]{1,0:T(8,128)(2,1)S(1)}) custom-call(bf16[128,256]{1,0:T(8,128)(2,1)} %query_hbm.1, bf16[128,256]{1,0:T(8,128)(2,1)} %key_hbm.1, bf16[128,256]{1,0:T(8,128)(2,1)} %value_hbm.1, f32[272,128]{1,0:T(8,128)} %constant.2.clone.table_hbm, f32[1,4]{1,0:T(1,128)} %bitcast.7, ...), custom_call_target="tpu_custom_call" | custom-call | tf_op jit(solution)/shard_map/pallas_call | solution.py:745
  34.1 0.7 %shard_map.141 = (bf16[32,2048]{1,0:T(8,128)(2,1)}, bf16[128,512]{1,0:T(8,128)(2,1)}) custom-call(bf16[32,2048]{1,0:T(8,128)(2,1)S(1)} %get-tuple-element.4.mixer_in, bf16[128,512]{1,0:T(8,128)(2,1)S(1)} %get-tuple-element.5.expert_in), custom_call_target="tpu_custom_call" | custom-call | tf_op jit(solution)/shard_map/pallas_call | solution.py:809

commit v4 on v3

--- a/solution.py
+++ b/solution.py
@@ -551,11 +551,19 @@
         for k, values in down_slice(number, owner):
             own_acc[p, k] = values
 
-    def cross(batch, places=range(quarter)):
-        base = batch[0]
+    def in_order(batch, places):
+        base, experts = batch
+        if places is not None or quarter % 2:
+            return [(base + i, experts[i]) for i in places or range(quarter)]
+        odd = lax.rem(me, 2)
+        return [
+            (base + i + odd * (j - i), experts[i] + odd * (experts[j] - experts[i]))
+            for i, j in [(i, i + 1 - 2 * (i % 2)) for i in range(quarter)]
+        ]
+
+    def cross(batch, places=None):
         for p in range(1, n_pair):
-            for i in places:
-                k = base + i
+            for k, _ in in_order(batch, places):
                 cross_send[p, k] = (own_acc[p, k] + sib_recv[p, k].astype(f32)).astype(bf16)
                 start(cross_copy(k, p))
 
@@ -563,10 +571,8 @@
         for p in parts:
             sib_copy(batch[0], p).wait_recv()
 
-    def finish(batch, places=range(quarter)):
-        base, experts = batch
-        for i in places:
-            k, expert = base + i, experts[i]
+    def finish(batch, places=None):
+        for k, expert in in_order(batch, places):
             total = own_acc[0, k] + sib_recv[0, k].astype(f32)
             for p in range(1, n_pair):
                 cross_copy(k, p).wait_recv()
@@ -624,21 +630,31 @@
         give(1, p)
         keep(1, p)
     give(1, 0)
-    met(far_batches[1], others)
-    cross(far_batches[1])
+    swap = middle * (1 - me // half_count)
+
+    def mixed(one, two):
+        return (
+            one[0] + swap * (two[0] - one[0]),
+            [first + swap * (second - first) for first, second in zip(one[1], two[1])],
+        )
+
+    sooner = mixed(far_batches[1], near_batches[1])
+    later = mixed(near_batches[1], far_batches[1])
+    met(sooner, others)
+    cross(sooner)
     met(far_batches[0], [0])
     finish(far_batches[0])
+    met(later, others)
+    cross(later)
     keep(1, 0)
-    met(near_batches[1], others)
-    cross(near_batches[1])
     cross(near_batches[0], [0])
     met(near_batches[0], [0])
     finish(near_batches[0], rest)
-    met(far_batches[1], [0])
-    finish(far_batches[1])
+    met(sooner, [0])
+    finish(sooner)
     mix_finish()
-    met(near_batches[1], [0])
-    finish(near_batches[1])
+    met(later, [0])
+    finish(later)
     finish(near_batches[0], [0])
 
     arrived(returned, final_recv_sem.at[0])

time: 35 us -> 33.5 us (0.957)
  the two profiles are of different devices: /device:TPU:0 before, /device:TPU:1 now
where the time goes in v4:
time: 33.5 us; the launch traced here: 33.3 us
  Pallas kernels  32.7 us (98%)
  between operations  0.64 us (2%)
    pallas_call x1, Pallas kernels, on_device(): pl.pallas_call(functools.partial(fused_kernel, (n_ep, n_tp, main, tail)),...  32 us
    pallas_call x1, Pallas kernels, on_device(): pl.pallas_call(write_kernel, out_shape=(jax.ShapeDtypeStruct(mixer_out.sh...  0.72 us

profile of v4, /device:TPU:1, one launch (start us, length us, event | category | flops | bytes accessed | tf_op | source)
XLA Modules:
  0.0 33.3 jit_solution(4630452449090499611)
XLA Ops:
  0.6 32.0 %shard_map.140 = (bf16[32,2048]{1,0:T(8,128)(2,1)S(1)}, bf16[128,512]{1,0:T(8,128)(2,1)S(1)}) custom-call(bf16[128,256]{1,0:T(8,128)(2,1)} %query_hbm.1, bf16[128,256]{1,0:T(8,128)(2,1)} %key_hbm.1, bf16[128,256]{1,0:T(8,128)(2,1)} %value_hbm.1, f32[272,128]{1,0:T(8,128)} %constant.2.clone.table_hbm, f32[1,4]{1,0:T(1,128)} %bitcast.7, ...), custom_call_target="tpu_custom_call" | custom-call | tf_op jit(solution)/shard_map/pallas_call | solution.py:761
  32.6 0.7 %shard_map.141 = (bf16[32,2048]{1,0:T(8,128)(2,1)}, bf16[128,512]{1,0:T(8,128)(2,1)}) custom-call(bf16[32,2048]{1,0:T(8,128)(2,1)S(1)} %get-tuple-element.4.mixer_in, bf16[128,512]{1,0:T(8,128)(2,1)S(1)} %get-tuple-element.5.expert_in), custom_call_target="tpu_custom_call" | custom-call | tf_op jit(solution)/shard_map/pallas_call | solution.py:825

commit v5 on v3

--- a/solution.py
+++ b/solution.py
@@ -144,10 +144,17 @@
         for place in (1, 0)
     ]
     far_batches = [(bases[place], far_experts[place]) for place in range(2)]
-    near_batches = [
-        (0, experts_of[:quarter]),
-        (quarter, experts_of[quarter:half_count]),
-    ]
+    swap = middle * (1 - me // half_count)
+
+    def mixed(one, two):
+        return (
+            one[0] + swap * (two[0] - one[0]),
+            [first + swap * (second - first) for first, second in zip(one[1], two[1])],
+        )
+
+    near_lists = [list(range(quarter)), list(range(quarter, half_count))]
+    near_pair = [(slots[0], [experts_of[k] for k in slots]) for slots in near_lists]
+    near_batches = [mixed(near_pair[0], near_pair[1]), mixed(near_pair[1], near_pair[0])]
     groups = [(far_batches[place], near_batches[place]) for place in range(2)]
     pair_up = [lax.rem(pair + p, n_pair) for p in range(n_pair)]
     pair_down = [lax.rem(pair + n_pair - p, n_pair) for p in range(n_pair)]
@@ -473,21 +480,29 @@
                 far_forward(base + i, p).wait_recv()
                 start(far_relay(base + i, p, number))
 
+    def either(number, action):
+        for swapped in range(2):
+            @pl.when(swap == swapped)
+            def _():
+                action([k for k in near_lists[(number + swapped) % 2] if k])
+
     def forward_near(number):
-        base, experts = near_batches[number]
-        for k in range(max(base, 1), base + len(experts)):
-            arrived(rows_in.at[pl.ds(0, n_pair), k], net_recv_sem.at[k])
-            for q in range(n_pair):
-                start(near_forward(k, q, 2 + number))
+        def action(slots):
+            for k in slots:
+                arrived(rows_in.at[pl.ds(0, n_pair), k], net_recv_sem.at[k])
+                for q in range(n_pair):
+                    start(near_forward(k, q, 2 + number))
+
+        either(number, action)
 
     def gather(number):
         slots = []
-        for kind, (base, experts) in enumerate(groups[number]):
-            count = len(experts)
-            slots += [base + i for i in range(count)]
-            if kind == 1 and number == 0:
-                count -= 1
-            arrived(rows_in.at[pl.ds(0, n_pair), pl.ds(0, count)], near_recv_sem.at[2 * kind + number])
+        for base, experts in groups[number]:
+            slots += [base + i for i in range(len(experts))]
+        arrived(rows_in.at[pl.ds(0, n_pair), pl.ds(0, quarter)], near_recv_sem.at[number])
+        either(number, lambda near: arrived(
+            rows_in.at[pl.ds(0, n_pair), pl.ds(0, len(near))], near_recv_sem.at[2 + number]
+        ))
         for owner in range(n_tp):
             for half in range(halves):
                 columns = pl.ds(owner * slice_width + half * piece, piece)
@@ -551,11 +566,23 @@
         for k, values in down_slice(number, owner):
             own_acc[p, k] = values
 
-    def cross(batch, places=range(quarter)):
-        base = batch[0]
+    def in_order(batch):
+        base, experts = batch
+        if quarter % 2:
+            return [(base + i, experts[i]) for i in range(quarter)]
+        odd = lax.rem(me, 2)
+        return [
+            (base + i + odd * (j - i), experts[i] + odd * (experts[j] - experts[i]))
+            for i, j in [(i, i + 1 - 2 * (i % 2)) for i in range(quarter)]
+        ]
+
+    outer = in_order(near_pair[1])
+    inner = [(k, experts_of[k]) for k in range(1, quarter)]
+    own = [(0, me)]
+
+    def cross(slots):
         for p in range(1, n_pair):
-            for i in places:
-                k = base + i
+            for k, _ in slots:
                 cross_send[p, k] = (own_acc[p, k] + sib_recv[p, k].astype(f32)).astype(bf16)
                 start(cross_copy(k, p))
 
@@ -563,10 +590,8 @@
         for p in parts:
             sib_copy(batch[0], p).wait_recv()
 
-    def finish(batch, places=range(quarter)):
-        base, experts = batch
-        for i in places:
-            k, expert = base + i, experts[i]
+    def finish(slots):
+        for k, expert in slots:
             total = own_acc[0, k] + sib_recv[0, k].astype(f32)
             for p in range(1, n_pair):
                 cross_copy(k, p).wait_recv()
@@ -595,12 +620,12 @@
             mixed += mix_recv[p].astype(f32)
         mixer_ref[...] = mixed.astype(mixer_ref.dtype)
 
-    others, rest = range(1, n_pair), range(1, quarter)
+    others = range(1, n_pair)
     forward_far(0)
-    forward_near(0)
     forward_far(1)
     relay_far(0)
     mix_forward()
+    forward_near(0)
     loads[9].wait()
     loads[10].wait()
     gather(0)
@@ -613,33 +638,43 @@
     for p in others:
         keep(0, p)
     give(0, 0)
+    def where(swapped, action, slots):
+        @pl.when(swap == swapped)
+        def _():
+            action(slots)
+
+    far_slots = [in_order(batch) for batch in far_batches]
     met(far_batches[0], others)
-    cross(far_batches[0])
+    cross(far_slots[0])
     keep(0, 0)
     gather(1)
     met(near_batches[0], others)
-    cross(near_batches[0], rest)
+    where(0, cross, inner)
+    where(1, cross, outer)
     expand()
     for p in others:
         give(1, p)
         keep(1, p)
     give(1, 0)
     met(far_batches[1], others)
-    cross(far_batches[1])
+    met(near_batches[1], others)
+    where(1, cross, inner)
+    cross(far_slots[1])
     met(far_batches[0], [0])
-    finish(far_batches[0])
+    finish(far_slots[0])
+    where(0, cross, outer)
+    cross(own)
     keep(1, 0)
-    met(near_batches[1], others)
-    cross(near_batches[1])
-    cross(near_batches[0], [0])
     met(near_batches[0], [0])
-    finish(near_batches[0], rest)
+    where(0, finish, inner)
+    where(1, finish, outer)
     met(far_batches[1], [0])
-    finish(far_batches[1])
+    met(near_batches[1], [0])
+    where(1, finish, inner)
+    finish(far_slots[1])
     mix_finish()
-    met(near_batches[1], [0])
-    finish(near_batches[1])
-    finish(near_batches[0], [0])
+    where(0, finish, outer)
+    finish(own)
 
     arrived(returned, final_recv_sem.at[0])
     blocks = returned[...].reshape(n_ep * blocked, piece)

time: 35 us -> 33.1 us (0.946)
  the two profiles are of different devices: /device:TPU:0 before, /device:TPU:11 now
where the time goes in v5:
time: 33.1 us; the launch traced here: 32.9 us
  Pallas kernels  32.3 us (98%)
  between operations  0.64 us (2%)
    pallas_call x1, Pallas kernels, on_device(): pl.pallas_call(functools.partial(fused_kernel, (n_ep, n_tp, main, tail)),...  31.6 us
    pallas_call x1, Pallas kernels, on_device(): pl.pallas_call(write_kernel, out_shape=(jax.ShapeDtypeStruct(mixer_out.sh...  0.72 us

profile of v5, /device:TPU:11, one launch (start us, length us, event | category | flops | bytes accessed | tf_op | source)
XLA Modules:
  0.0 32.9 jit_solution(12312063149191595809)
XLA Ops:
  0.6 31.6 %shard_map.140 = (bf16[32,2048]{1,0:T(8,128)(2,1)S(1)}, bf16[128,512]{1,0:T(8,128)(2,1)S(1)}) custom-call(bf16[128,256]{1,0:T(8,128)(2,1)} %query_hbm.1, bf16[128,256]{1,0:T(8,128)(2,1)} %key_hbm.1, bf16[128,256]{1,0:T(8,128)(2,1)} %value_hbm.1, f32[272,128]{1,0:T(8,128)} %constant.2.clone.table_hbm, f32[1,4]{1,0:T(1,128)} %bitcast.7, ...), custom_call_target="tpu_custom_call" | custom-call | tf_op jit(solution)/shard_map/pallas_call | solution.py:780
  32.2 0.7 %shard_map.141 = (bf16[32,2048]{1,0:T(8,128)(2,1)}, bf16[128,512]{1,0:T(8,128)(2,1)}) custom-call(bf16[32,2048]{1,0:T(8,128)(2,1)S(1)} %get-tuple-element.4.mixer_in, bf16[128,512]{1,0:T(8,128)(2,1)S(1)} %get-tuple-element.5.expert_in), custom_call_target="tpu_custom_call" | custom-call | tf_op jit(solution)/shard_map/pallas_call | solution.py:844

commit v6 on v5

--- a/solution.py
+++ b/solution.py
@@ -441,14 +441,17 @@
             jnp.where(number < 2 * main + tail, number - main, number - main - tail),
         )
         left = (number < main) | (jnp.logical_not(in_main) & (number < 2 * main + tail))
+    lefts, rights = [], []
     for k in range(n_ep):
         placed = jnp.zeros((blocked, row_count), f32)
         for j in range(TOP):
             chosen = jnp.where(routes[j] == experts_of[k], rank[j], -1) == slot_of
             placed = jnp.where(chosen, route_weight_v[j : j + 1, :], placed)
-        combine_left[pl.ds(k * blocked, blocked)] = jnp.where(left, placed, 0.0).astype(bf16)
-        if tail:
-            combine_right[pl.ds(k * blocked, blocked)] = jnp.where(left, 0.0, placed).astype(bf16)
+        lefts.append(jnp.where(left, placed, 0.0))
+        rights.append(jnp.where(left, 0.0, placed))
+    combine_left[...] = jnp.concatenate(lefts, axis=0).T.astype(bf16)
+    if tail:
+        combine_right[...] = jnp.concatenate(rights, axis=0).T.astype(bf16)
 
     def near_forward(k, q, sem):
         owner = 2 * pair_up[q] + 1 - core
@@ -681,7 +684,7 @@
 
     def combined(weights_ref):
         return lax.dot_general(
-            weights_ref[...], blocks, (((0,), (0,)), ((), ())), preferred_element_type=f32
+            weights_ref[...], blocks, (((1,), (0,)), ((), ())), preferred_element_type=f32
         )
 
     expert_ref[:, :piece] = combined(combine_left).astype(expert_ref.dtype)
@@ -819,8 +822,8 @@
             pltpu.VMEM((n_pair, n_ep) + traveling, bf16),
             pltpu.VMEM((n_ep,) + traveling, bf16),
             pltpu.VMEM((n_ep,) + traveling, bf16),
-            pltpu.VMEM((n_ep * blocked, row_count), bf16),
-            pltpu.VMEM((n_ep * blocked, row_count), bf16),
+            pltpu.VMEM((row_count, n_ep * blocked), bf16),
+            pltpu.VMEM((row_count, n_ep * blocked), bf16),
             dma((13,)),
             dma((2,)),
             dma((2,)),

time: 33.1 us -> 33.3 us (level)
  the two profiles are of different devices: /device:TPU:11 before, /device:TPU:0 now
where the time goes in v6:
time: 33.3 us; the launch traced here: 32.8 us
  Pallas kernels  32.2 us (97%)
  between operations  0.64 us (2%)
    pallas_call x1, Pallas kernels, on_device(): pl.pallas_call(functools.partial(fused_kernel, (n_ep, n_tp, main, tail)),...  31.4 us
    pallas_call x1, Pallas kernels, on_device(): pl.pallas_call(write_kernel, out_shape=(jax.ShapeDtypeStruct(mixer_out.sh...  0.72 us

profile of v6, /device:TPU:0, one launch (start us, length us, event | category | flops | bytes accessed | tf_op | source)
XLA Modules:
  0.0 32.8 jit_solution(17928730192952522580)
XLA Ops:
  0.6 31.4 %shard_map.140 = (bf16[32,2048]{1,0:T(8,128)(2,1)S(1)}, bf16[128,512]{1,0:T(8,128)(2,1)S(1)}) custom-call(bf16[128,256]{1,0:T(8,128)(2,1)} %query_hbm.1, bf16[128,256]{1,0:T(8,128)(2,1)} %key_hbm.1, bf16[128,256]{1,0:T(8,128)(2,1)} %value_hbm.1, f32[272,128]{1,0:T(8,128)} %constant.2.clone.table_hbm, f32[1,4]{1,0:T(1,128)} %bitcast.7, ...), custom_call_target="tpu_custom_call" | custom-call | tf_op jit(solution)/shard_map/pallas_call | solution.py:783
  32.1 0.7 %shard_map.141 = (bf16[32,2048]{1,0:T(8,128)(2,1)}, bf16[128,512]{1,0:T(8,128)(2,1)}) custom-call(bf16[32,2048]{1,0:T(8,128)(2,1)S(1)} %get-tuple-element.4.mixer_in, bf16[128,512]{1,0:T(8,128)(2,1)S(1)} %get-tuple-element.5.expert_in), custom_call_target="tpu_custom_call" | custom-call | tf_op jit(solution)/shard_map/pallas_call | solution.py:847
